TPU v7x, 32 devices: a whole 2x2x4 slice. The times are simulated.
32 devices in a mesh: sp: 16 (over z, y, core), tp: 2 (over x).
Axes of the slice: x: 2, y: 2, z: 4, core: 2. Of those that a mesh axis runs over, the one named last changes fastest.
Arguments:
- queries: bfloat16 [16384, 1024], P('sp', 'tp'), may hold values from -8 to 8
- keys: bfloat16 [16384, 256], P('sp', 'tp'), may hold values from -8 to 8
- values: bfloat16 [16384, 256], P('sp', 'tp'), may hold values from -18 to 18
- doc_ids: int32 [16384], P('sp'), may hold values from 0 to 3, never falling along the last dimension, each value on 1 to 8192 neighbouring positions
- sinks: float32 [16], P('tp'), may hold values from 0 to 4
- residual: bfloat16 [16384, 2048], P(('sp', 'tp')), may hold values from -12 to 12
- out_weight: bfloat16 [1024, 2048], P('tp'), may hold values from -0.1875 to 0.1875
- norm_gain: float32 [2048], replicated, may hold values from 0.1 to 1.9
- w_gate: bfloat16 [2048, 5632], P('sp', 'tp'), may hold values from -0.125 to 0.125
- w_value: bfloat16 [2048, 5632], P('sp', 'tp'), may hold values from -0.125 to 0.125
- conv_gate: float32 [3, 5632], P(None, 'tp'), may hold values from -3.5 to 3.5
- conv_value: float32 [3, 5632], P(None, 'tp'), may hold values from -3.5 to 3.5
- w_down: bfloat16 [5632, 2048], P('tp', 'sp'), may hold values from -0.078125 to 0.078125
Outputs:
- layer_out: bfloat16 [16384, 2048], P(('sp', 'tp'))
All inputs are finite; a program needn't handle non-finite values.
Results may differ from a plain program's by a relative error of at most 0.012.
Values may be sent and summed in bfloat16 or wider, within the bound.
A program may use at most 128 MiB of HBM per device.

v0:
```python
import functools

import jax
import jax.numpy as jnp
from jax import lax
from jax.experimental import pallas as pl
from jax.experimental.pallas import tpu as pltpu
from jax.sharding import PartitionSpec as P


HEAD_DIM = 64
WINDOW = 128
ROW_TILE = 128
SUB = 2
HALO = 16
TILE = 256
VMEM_BYTES = 67043328
MESH = pl.DeviceIdType.MESH


def shifted(shard, axis, by):
    size = lax.axis_size(axis)
    pairs = [(i, i + by) for i in range(size) if 0 <= i + by < size]
    return lax.ppermute(shard, axis, pairs)


def turned(t, axis, by):
    size = lax.axis_size(axis)
    return lax.ppermute(t, axis, [(i, (i + by) % size) for i in range(size)])


def core_swap(t):
    size = lax.axis_size("sp")
    return lax.ppermute(t, "sp", [(i, i ^ 1) for i in range(size)])


def parity_gather(t):
    size = lax.axis_size("sp")
    groups = [list(range(0, size, 2)), list(range(1, size, 2))]
    return lax.all_gather(t, "sp", axis=0, tiled=True, axis_index_groups=groups)


def ring_gather(t):
    chips = lax.axis_size("sp") // 2
    order = list(range(0, chips, 2)) + list(range(1, chips, 2))[::-1]
    chip = lax.axis_index("sp") // 2
    place = jnp.where(chip % 2 == 0, chip // 2, chips - 1 - chip // 2)

    def hop(piece, by):
        pairs = [
            (2 * order[k] + c, 2 * order[(k + by) % chips] + c)
            for k in range(chips)
            for c in range(2)
        ]
        return lax.ppermute(piece, "sp", pairs)

    def chip_at(k):
        k = (k + chips) % chips
        return jnp.where(k < chips // 2, 2 * k, 2 * (chips - 1 - k) + 1)

    depth = t.shape[0]
    pieces = [(chip, t)]
    up = down = t
    for step in range(1, chips // 2 + 1):
        up = hop(up, 1)
        pieces.append((chip_at(place - step), up))
        if step < chips - step:
            down = hop(down, -1)
            pieces.append((chip_at(place + step), down))
    whole = jnp.zeros((chips * depth,) + t.shape[1:], t.dtype)
    for at, piece in pieces:
        whole = lax.dynamic_update_slice_in_dim(whole, piece, at * depth, 0)
    return whole


def by_parity(t, depth):
    rows, width = t.shape
    blocks = width // depth
    tile = min(ROW_TILE, rows)

    def kernel(in_ref, out_ref):
        for j in range(blocks):
            to = (j // 2 + (j % 2) * (blocks // 2)) * depth
            out_ref[:, to : to + depth] = in_ref[:, j * depth : (j + 1) * depth]

    return pl.pallas_call(
        kernel,
        out_shape=jax.ShapeDtypeStruct(t.shape, t.dtype),
        grid=(rows // tile,),
        in_specs=[pl.BlockSpec((tile, width), lambda i: (i, 0))],
        out_specs=pl.BlockSpec((tile, width), lambda i: (i, 0)),
        cost_estimate=pl.CostEstimate(
            flops=0, bytes_accessed=2 * t.size * t.dtype.itemsize, transcendentals=0
        ),
    )(t)


def finish(mid, sums, depth):
    rows, width = mid.shape
    blocks = width // depth
    tile = min(ROW_TILE, rows)

    def kernel(mid_ref, even_ref, odd_ref, out_ref):
        for j in range(blocks):
            at = (j // 2) * depth
            held = at + (j % 2) * (width // 2)
            sum_ref = odd_ref if j % 2 else even_ref
            out_ref[:, j * depth : (j + 1) * depth] = (
                mid_ref[:, held : held + depth].astype(jnp.float32)
                + sum_ref[:, at : at + depth]
            ).astype(out_ref.dtype)

    half_spec = pl.BlockSpec((tile, width // 2), lambda i: (i, 0))
    return pl.pallas_call(
        kernel,
        out_shape=jax.ShapeDtypeStruct(mid.shape, mid.dtype),
        grid=(rows // tile,),
        in_specs=[pl.BlockSpec((tile, width), lambda i: (i, 0)), half_spec, half_spec],
        out_specs=pl.BlockSpec((tile, width), lambda i: (i, 0)),
        cost_estimate=pl.CostEstimate(
            flops=mid.size, bytes_accessed=8 * mid.size, transcendentals=0
        ),
    )(mid, *sums)


def attend(query_rows, key_ext, value_ext, doc_rows, doc_ext, sinks):
    row_count = query_rows.shape[0]
    block_count = row_count // WINDOW
    kv_heads = key_ext.shape[1] // HEAD_DIM
    group_size = query_rows.shape[1] // (kv_heads * HEAD_DIM)

    def band(t):
        lower = t[:row_count].reshape((block_count, WINDOW) + t.shape[1:])
        upper = t[WINDOW:].reshape((block_count, WINDOW) + t.shape[1:])
        return jnp.concatenate([lower, upper], axis=1)

    query_band = query_rows.reshape(block_count, WINDOW, kv_heads, group_size, HEAD_DIM)
    key_band = band(key_ext).reshape(block_count, 2 * WINDOW, kv_heads, HEAD_DIM)
    value_band = band(value_ext).reshape(block_count, 2 * WINDOW, kv_heads, HEAD_DIM)
    doc_band = band(doc_ext)
    distance = jnp.arange(WINDOW)[:, None] + WINDOW - jnp.arange(2 * WINDOW)[None, :]
    in_window = (distance >= 0) & (distance < WINDOW)
    same_doc = doc_rows.reshape(block_count, WINDOW)[:, :, None] == doc_band[:, None, :]
    keep_mask = in_window[None] & same_doc
    scores = jnp.einsum(
        "nqhgd,nkhd->nhgqk", query_band, key_band, preferred_element_type=jnp.float32
    ) * HEAD_DIM ** (-0.5)
    scores = jnp.where(keep_mask[:, None, None], scores, -jnp.inf)
    sink_logit = sinks.reshape(kv_heads, group_size)[None, :, :, None, None]
    peak = jnp.maximum(jnp.max(scores, axis=-1, keepdims=True), sink_logit)
    expd = jnp.exp(scores - peak)
    probs = (expd / (jnp.sum(expd, axis=-1, keepdims=True) + jnp.exp(sink_logit - peak))).astype(
        jnp.bfloat16
    )
    mixed = jnp.einsum("nhgqk,nkhd->nqhgd", probs, value_band, preferred_element_type=jnp.float32)
    return mixed.astype(jnp.bfloat16).reshape(row_count, -1)


def convolve(ext_rows, doc_ext, taps):
    center = doc_ext[2:]
    same_one = (doc_ext[1:-1] == center)[:, None]
    same_two = (doc_ext[:-2] == center)[:, None]
    ext32 = ext_rows.astype(jnp.float32)
    result = taps[2] * ext32[2:]
    result = result + jnp.where(same_one, taps[1] * ext32[1:-1], 0.0)
    return result + jnp.where(same_two, taps[0] * ext32[:-2], 0.0)


def per_device(
    queries,
    keys,
    values,
    doc_ids,
    sinks,
    residual,
    out_weight,
    norm_gain,
    w_gate,
    w_value,
    conv_gate,
    conv_value,
    w_down,
):
    core = lax.axis_index("sp") % 2
    tp = lax.axis_index("tp")
    n_tp = lax.axis_size("tp")
    rows = doc_ids.shape[0]
    part_rows = rows // n_tp
    depth = w_gate.shape[0]
    width = residual.shape[1]
    half = width // 2
    part_index = [(tp + n_tp - d) % n_tp for d in range(n_tp)]

    gate_own = parity_gather(w_gate)
    value_own = ring_gather(w_value)
    down_t = w_down.T
    inner = down_t.shape[1] // 2
    low, high = down_t[:, :inner], down_t[:, inner:]
    kept_half = jnp.where(core == 0, low, high)
    came_half = core_swap(jnp.where(core == 0, high, low))
    even_piece = jnp.where(core == 0, kept_half, came_half)
    odd_piece = jnp.where(core == 0, came_half, kept_half)
    down_odd = parity_gather(odd_piece)
    down_even = parity_gather(even_piece)
    gate_far = core_swap(gate_own)
    value_far = core_swap(value_own)

    out_far = [turned(out_weight, "tp", d) for d in range(1, n_tp)]
    out_parts = [by_parity(t, depth) for t in [out_weight] + out_far]
    residual = by_parity(residual, depth)
    norm_gain = norm_gain.reshape(-1, 2, depth).swapaxes(0, 1).reshape(-1)
    docs_plus = doc_ids + 1
    prev_keys, prev_values, prev_docs = shifted(
        (keys[-WINDOW:], values[-WINDOW:], docs_plus[-WINDOW:]), "sp", 1
    )
    key_ext = jnp.concatenate([prev_keys, keys], axis=0)
    value_ext = jnp.concatenate([prev_values, values], axis=0)
    doc_ext = jnp.concatenate([prev_docs, docs_plus], axis=0)
    head_out = attend(queries, key_ext, value_ext, docs_plus, doc_ext, sinks)

    def rows_of(t, index):
        return lax.dynamic_slice_in_dim(t, index * part_rows, part_rows, 0)

    proj = jnp.dot(rows_of(head_out, tp), out_parts[0], preferred_element_type=jnp.float32)
    for d in range(1, n_tp):
        heads_far = turned(rows_of(head_out, (tp + d) % n_tp), "tp", d)
        proj = proj + jnp.dot(heads_far, out_parts[d], preferred_element_type=jnp.float32)
    mid = (residual.astype(jnp.float32) + proj).astype(jnp.bfloat16)
    mid32 = mid.astype(jnp.float32)
    normed = (
        mid32 * lax.rsqrt(jnp.mean(mid32 * mid32, axis=-1, keepdims=True) + 1e-06) * norm_gain
    ).astype(jnp.bfloat16)
    even, odd = normed[:, :half], normed[:, half:]
    own = [jnp.where(core == 0, even, odd)]
    far = [jnp.where(core == 0, odd, even)]
    for d in range(1, n_tp):
        own.append(turned(own[0], "tp", d))
        far.append(turned(far[0], "tp", d))

    def up(own, far, w_own, w_far):
        total = jnp.dot(own, w_own, preferred_element_type=jnp.float32)
        return (total + jnp.dot(far, w_far, preferred_element_type=jnp.float32)).astype(
            jnp.bfloat16
        )

    gate_parts = [up(o, f, gate_own, gate_far) for o, f in zip(own, far)]
    value_parts = [up(o, f, value_own, value_far) for o, f in zip(own, far)]

    conv_docs = jnp.concatenate([prev_docs[-2:], docs_plus], axis=0)
    part_docs = [
        lax.dynamic_slice_in_dim(conv_docs, i * part_rows, part_rows + 2, 0) for i in part_index
    ]

    def conv_parts(parts, taps):
        tails = [p[-2:] for p in parts]
        last = tails[0]
        for d in range(1, n_tp):
            last = jnp.where(part_index[d] == n_tp - 1, tails[d], last)
        prev = shifted(last, "sp", 1)
        result = []
        for d in range(n_tp):
            halo = jnp.where(part_index[d] == 0, prev, tails[(d + 1) % n_tp])
            result.append(
                convolve(jnp.concatenate([halo, parts[d]], axis=0), part_docs[d], taps)
            )
        return result

    gate_conv = conv_parts(gate_parts, conv_gate)
    value_conv = conv_parts(value_parts, conv_value)
    hidden = [
        (jax.nn.silu(g) * v).astype(jnp.bfloat16) for g, v in zip(gate_conv, value_conv)
    ]

    def down(units, w_t):
        return lax.dot_general(
            units, w_t, (((1,), (1,)), ((), ())), preferred_element_type=jnp.float32
        )

    own_units = [jnp.where(core == 0, h[:, :inner], h[:, inner:]) for h in hidden]
    far_units = [jnp.where(core == 0, h[:, inner:], h[:, :inner]) for h in hidden]

    def down_sums(w_own):
        w_far = core_swap(w_own)
        came = []
        for d in range(1, n_tp):
            sent = (down(own_units[d], w_own) + down(far_units[d], w_far)).astype(
                jnp.bfloat16
            )
            came.append(turned(sent, "tp", -d))
        kept = down(own_units[0], w_own) + down(far_units[0], w_far)
        for t in came:
            kept = kept + t.astype(jnp.float32)
        return kept

    odd_sum = down_sums(down_odd)
    even_sum = down_sums(down_even)
    sums = (even_sum, odd_sum)
    return finish(mid, sums, depth)


def mult(x, m):
    return x if isinstance(x, int) else pl.multiple_of(x, m)


def ring_chip(place, chips):
    odd = lax.div(place, chips // 2)
    return (1 - odd) * (2 * place) + odd * (2 * (chips - 1 - place) + 1)


def layer_kernel(
    n_sp,
    n_tp,
    queries,
    keys,
    values,
    docs,
    sinks,
    residual,
    out_weight,
    norm_gain,
    w_gate,
    w_value,
    conv_gate,
    conv_value,
    w_down,
    out,
    wg,
    wv,
    wd,
    nrm,
    hid,
    pre,
    q_v,
    k_v,
    v_v,
    doc_v,
    doc_col,
    same_one,
    same_two,
    att,
    heads,
    ow,
    mid,
    gain_v,
    cg_v,
    cv_v,
    send,
    came,
    own,
    local_sem,
    ring_send,
    ring_recv,
    sib_send,
    sib_recv,
    halo_send,
    halo_recv,
    ow_send,
    ow_recv,
    heads_send,
    heads_recv,
    nrm_send,
    nrm_recv,
    sum_send,
    sum_recv,
    out_sem,
):
    sp = lax.axis_index("sp")
    tp = lax.axis_index("tp")
    chips = n_sp // 2
    core = lax.rem(sp, 2)
    chip = lax.div(sp, 2)
    odd = lax.rem(chip, 2)
    place = (1 - odd) * lax.div(chip, 2) + odd * (chips - 1 - lax.div(chip, 2))
    way = 1 - 2 * core
    down_sp = 2 * ring_chip(lax.rem(place + way + chips, chips), chips) + core
    up_sp = 2 * ring_chip(lax.rem(place - way + chips, chips), chips) + core
    sib_sp = sp + way
    next_sp = lax.rem(sp + 1, n_sp)
    prev_sp = lax.rem(sp + n_sp - 1, n_sp)

    rows, q_width = queries.shape
    part = rows // n_tp
    depth, units = w_gate.shape
    kv_heads = keys.shape[1] // HEAD_DIM
    group = q_width // keys.shape[1]
    blocks = rows // WINDOW
    part_blocks = part // WINDOW
    ow_half = q_width // 2
    unit_tiles = units // TILE
    events = (chips - 1) * SUB

    def peer(d):
        return lax.rem(tp + d, n_tp)

    def held(h):
        return 2 * ring_chip(lax.rem(place - way * h + chips, chips), chips) + core

    def sib_held(h):
        return 2 * ring_chip(lax.rem(place + way * h + chips, chips), chips) + 1 - core

    def piece(w, j, s):
        if w == 2:
            size = units // SUB
            return wd.at[j, pl.ds(mult(s * size, size), size), :]
        size = depth // SUB
        buf = (wg, wv)[w]
        return buf.at[pl.ds(mult(j * depth + s * size, size), size), :]

    def own_piece(w, s):
        ref = (w_gate, w_value, w_down)[w]
        size = ref.shape[0] // SUB
        return ref.at[pl.ds(s * size, size), :]

    def remote(src, dst, send_sem, recv_sem, device):
        return pltpu.make_async_remote_copy(
            src_ref=src,
            dst_ref=dst,
            send_sem=send_sem,
            recv_sem=recv_sem,
            device_id=device,
            device_id_type=MESH,
        )

    def ring_copy(w, h, s, src=None):
        dst = piece(w, held(h - 1), s)
        return remote(
            dst if src is None else src,
            dst,
            ring_send.at[w, h, s],
            ring_recv.at[w, h, s],
            (down_sp, tp),
        )

    def ring_wait(w, h, s):
        dst = piece(w, held(h), s)
        remote(
            dst, dst, ring_send.at[w, h, s], ring_recv.at[w, h, s], (down_sp, tp)
        ).wait_recv()

    def sib_copy(w, h, s, src=None):
        dst = piece(w, held(h), s)
        return remote(
            dst if src is None else src,
            dst,
            sib_send.at[w, h, s],
            sib_recv.at[w, h, s],
            (sib_sp, tp),
        )

    def sib_wait(w, h, s):
        dst = piece(w, sib_held(h), s)
        remote(
            dst, dst, sib_send.at[w, h, s], sib_recv.at[w, h, s], (sib_sp, tp)
        ).wait_recv()

    def start_own(w):
        for s in range(SUB):
            ring_copy(w, 1, s, own_piece(w, s)).start()
        for s in range(SUB):
            sib_copy(w, 0, s, own_piece(w, s)).start()

    def service(w, e):
        h = 1 + (e // SUB if isinstance(e, int) else lax.div(e, SUB))
        s = e % SUB if isinstance(e, int) else lax.rem(e, SUB)
        ring_wait(w, h, s)
        if isinstance(e, int):
            if h < chips - 1:
                ring_copy(w, h + 1, s).start()
        else:

            @pl.when(h < chips - 1)
            def _():
                ring_copy(w, h + 1, s).start()

        sib_copy(w, h, s).start()

    def serve(w, first, last):
        if last > first:

            @pl.loop(first, last)
            def _(e):
                service(w, e)

    local = [
        (keys, k_v.at[pl.ds(WINDOW, rows), :]),
        (values, v_v.at[pl.ds(WINDOW, rows), :]),
        (docs, doc_v.at[pl.ds(8, blocks), :]),
        (queries, q_v),
        (residual, mid),
        (out_weight, ow.at[tp]),
        (norm_gain, gain_v),
        (conv_gate, cg_v),
        (conv_value, cv_v),
        (w_gate, wg.at[pl.ds(mult(sp * depth, depth), depth), :]),
        (w_value, wv.at[pl.ds(mult(sp * depth, depth), depth), :]),
        (w_down, wd.at[sp]),
    ]
    local = [
        pltpu.make_async_copy(src, dst, local_sem.at[i]) for i, (src, dst) in enumerate(local)
    ]
    for copy in local:
        copy.start()

    barrier = pltpu.get_barrier_semaphore()
    greeted = [(down_sp, tp), (up_sp, tp), (sib_sp, tp), (next_sp, tp), (prev_sp, tp)]
    greeted += [(sp, peer(d)) for d in range(1, n_tp)]
    for device in greeted:
        pl.semaphore_signal(barrier, inc=1, device_id=device, device_id_type=MESH)
    pl.semaphore_wait(barrier, len(greeted))

    halos = [
        (keys.at[pl.ds(rows - WINDOW, WINDOW), :], k_v.at[pl.ds(0, WINDOW), :]),
        (values.at[pl.ds(rows - WINDOW, WINDOW), :], v_v.at[pl.ds(0, WINDOW), :]),
        (docs.at[pl.ds(blocks - 1, 1), :], doc_v.at[pl.ds(7, 1), :]),
    ]
    halos = [
        remote(src, dst, halo_send.at[i], halo_recv.at[i], (next_sp, tp))
        for i, (src, dst) in enumerate(halos)
    ]
    for copy in halos:
        copy.start()
    start_own(0)

    def ow_rows(t, c):
        return ow.at[t, pl.ds(mult(c * ow_half, ow_half), ow_half), :]

    ow_src = out_weight.at[pl.ds(mult(core * ow_half, ow_half), ow_half), :]
    ow_out = [
        remote(ow_src, ow_rows(tp, core), ow_send.at[0, d], ow_recv.at[0, d], (sp, peer(n_tp - d)))
        for d in range(1, n_tp)
    ]
    for copy in ow_out:
        copy.start()

    for i in range(3):
        local[i].wait()
    for copy in halos:
        copy.wait_recv()
    local[3].wait()

    lane = lax.broadcasted_iota(jnp.int32, (WINDOW, 2 * HEAD_DIM), 1)
    low_lane = lane < HEAD_DIM
    doc_v[7:8, :] = jnp.where(sp == 0, 0, doc_v[7:8, :])
    for b in range(-1, blocks):
        row = doc_v[8 + b : 9 + b, :]
        column = jnp.broadcast_to(row, (WINDOW, WINDOW)).T
        if b < 0:
            doc_col[0:8, :] = column[WINDOW - 8 :, :]
        else:
            doc_col[8 + b * WINDOW : 8 + (b + 1) * WINDOW, :] = column
    for b in range(blocks):
        at = 8 + b * WINDOW
        here = doc_col[at : at + WINDOW, :]
        back_one = doc_col[at - 1 : at - 1 + WINDOW, :]
        back_two = doc_col[at - 2 : at - 2 + WINDOW, :]
        to = slice(b * WINDOW, (b + 1) * WINDOW)
        same_one[to, :] = jnp.where(here == back_one, 1.0, 0.0)
        same_two[to, :] = jnp.where(here == back_two, 1.0, 0.0)

    q_index = lax.broadcasted_iota(jnp.int32, (WINDOW, 2 * WINDOW), 0)
    k_index = lax.broadcasted_iota(jnp.int32, (WINDOW, 2 * WINDOW), 1)
    first_rows = lax.broadcasted_iota(jnp.int32, (2 * WINDOW, 1), 0) < WINDOW

    def attend_block(b):
        base = mult(b * WINDOW, WINDOW)
        key_docs = jnp.concatenate([doc_v[pl.ds(7 + b, 1), :], doc_v[pl.ds(8 + b, 1), :]], axis=1)
        here = doc_col[pl.ds(mult(8 + base, 8), WINDOW), :]
        keep = (k_index > q_index) & (k_index <= q_index + WINDOW)
        keep = keep & (jnp.concatenate([here, here], axis=1) == key_docs)
        keep = jnp.concatenate([keep, keep], axis=0)
        k_band = k_v[pl.ds(base, 2 * WINDOW), :]
        v_band = v_v[pl.ds(base, 2 * WINDOW), :]
        for g in range(kv_heads):
            at = slice(g * HEAD_DIM, (g + 1) * HEAD_DIM)
            kk = jnp.concatenate([k_band[:, at], k_band[:, at]], axis=1)
            vv = jnp.concatenate([v_band[:, at], v_band[:, at]], axis=1)
            for pair in range(group // 2):
                head = g * group + 2 * pair
                lanes = slice(head * HEAD_DIM, (head + 2) * HEAD_DIM)
                both = q_v[pl.ds(base, WINDOW), lanes]
                zero = jnp.zeros_like(both)
                split = jnp.concatenate(
                    [jnp.where(low_lane, both, zero), jnp.where(low_lane, zero, both)], axis=0
                )
                scores = lax.dot_general(
                    split, kk, (((1,), (1,)), ((), ())), preferred_element_type=jnp.float32
                ) * HEAD_DIM ** (-0.5)
                scores = jnp.where(keep, scores, -1e30)
                sink = jnp.where(first_rows, sinks[head], sinks[head + 1])
                peak = jnp.maximum(jnp.max(scores, axis=1, keepdims=True), sink)
                expd = jnp.exp(scores - peak)
                total = jnp.sum(expd, axis=1, keepdims=True) + jnp.exp(sink - peak)
                probs = (expd * (1.0 / total)).astype(jnp.bfloat16)
                mixed = jnp.dot(probs, vv, preferred_element_type=jnp.float32)
                att[pl.ds(base, WINDOW), lanes] = jnp.where(
                    low_lane, mixed[:WINDOW], mixed[WINDOW:]
                ).astype(jnp.bfloat16)

    early = events // 7
    pl.loop(0, blocks - part_blocks)(
        lambda i: attend_block(lax.rem((tp + 1) * part_blocks + i, blocks))
    )
    serve(0, 0, early // 2)
    pl.loop(0, part_blocks)(lambda i: attend_block(tp * part_blocks + i))
    heads_out = [
        remote(
            att.at[pl.ds(mult(peer(n_tp - d) * part, part), part), :],
            heads.at[d - 1],
            heads_send.at[d],
            heads_recv.at[d],
            (sp, peer(n_tp - d)),
        )
        for d in range(1, n_tp)
    ]
    for copy in heads_out:
        copy.start()
    before_proj = 3 * early
    serve(0, early // 2, before_proj)

    for i in range(4, 9):
        local[i].wait()
    ow_on = []
    for d in range(1, n_tp):
        got = ow_rows(peer(d), core)
        remote(got, got, ow_send.at[0, d], ow_recv.at[0, d], (sp, peer(n_tp - d))).wait_recv()
        copy = remote(got, got, ow_send.at[1, d], ow_recv.at[1, d], (sib_sp, tp))
        copy.start()
        ow_on.append(copy)
    for d in range(1, n_tp):
        got = ow_rows(peer(d), 1 - core)
        remote(got, got, ow_send.at[1, d], ow_recv.at[1, d], (sib_sp, tp)).wait_recv()
        heads_out[d - 1].wait_recv()

    part_base = tp * part

    def nrm_rows(t, i):
        return nrm.at[pl.ds(mult(HALO + t * part + i * WINDOW, HALO), WINDOW), :]

    def nrm_copy(i, d):
        at = nrm_rows(tp, i)
        return remote(at, at, nrm_send.at[i, d], nrm_recv.at[i, d], (sp, peer(n_tp - d)))

    def project(i):
        at = pl.ds(mult(i * WINDOW, WINDOW), WINDOW)
        mine = att[pl.ds(mult(part_base + i * WINDOW, WINDOW), WINDOW), :]
        proj = jnp.dot(mine, ow[tp], preferred_element_type=jnp.float32)
        for d in range(1, n_tp):
            proj = proj + jnp.dot(
                heads[d - 1, at, :], ow[peer(d)], preferred_element_type=jnp.float32
            )
        rounded = (mid[at, :].astype(jnp.float32) + proj).astype(jnp.bfloat16)
        mid[at, :] = rounded
        wide = rounded.astype(jnp.float32)
        scale = lax.rsqrt(jnp.mean(wide * wide, axis=1, keepdims=True) + 1e-06)
        normed = (wide * scale * gain_v[...]).astype(jnp.bfloat16)
        nrm[pl.ds(mult(HALO + part_base + i * WINDOW, HALO), WINDOW), :] = normed

    @pl.loop(0, part_blocks)
    def _(i):
        project(i)
        for d in range(1, n_tp):

            @pl.when(i > 0)
            def _():
                nrm_copy(i - 1, d).start()

        @pl.when(before_proj + i < events)
        def _():
            service(0, before_proj + i)

    for d in range(1, n_tp):
        nrm_copy(part_blocks - 1, d).start()

    after_proj = min(events, before_proj + part_blocks)
    serve(0, after_proj, events)
    start_own(1)
    early_value = 2 * early
    serve(1, 0, early_value)

    @pl.loop(0, part_blocks)
    def _(i):
        for d in range(1, n_tp):
            got = nrm_rows(peer(d), i)
            remote(
                got, got, nrm_send.at[i, d], nrm_recv.at[i, d], (sp, peer(n_tp - d))
            ).wait_recv()

    nrm_halo = remote(
        nrm.at[pl.ds(rows, HALO), :],
        nrm.at[pl.ds(0, HALO), :],
        halo_send.at[3],
        halo_recv.at[3],
        (next_sp, tp),
    )
    nrm_halo.start()
    for i in range(9, 12):
        local[i].wait()

    def all_of_sib(w):
        @pl.loop(0, chips * SUB)
        def _(e):
            sib_wait(w, lax.div(e, SUB), lax.rem(e, SUB))

    all_of_sib(0)
    nrm_halo.wait_recv()

    half_rows = HALO + rows // 2

    def up_tile(w_ref, taps, n):
        cols = pl.ds(mult(n * TILE, TILE), TILE)
        for lo, hi in ((0, half_rows), (half_rows, HALO + rows)):
            pre[lo:hi, :] = (
                jnp.dot(nrm[lo:hi, :], w_ref[:, cols], preferred_element_type=jnp.float32)
                .astype(jnp.bfloat16)
                .astype(jnp.float32)
            )
        tap = taps[:, cols]
        for b in range(blocks):
            at = HALO + b * WINDOW
            to = slice(b * WINDOW, (b + 1) * WINDOW)
            one = jnp.concatenate([same_one[to, :]] * (TILE // WINDOW), axis=1)
            two = jnp.concatenate([same_two[to, :]] * (TILE // WINDOW), axis=1)
            conv = tap[2:3] * pre[at : at + WINDOW, :]
            conv = conv + one * (tap[1:2] * pre[at - 1 : at - 1 + WINDOW, :])
            conv = conv + two * (tap[0:1] * pre[at - 2 : at - 2 + WINDOW, :])
            yield to, cols, conv

    def spread(w, first, count, i):
        before = lax.div(i * count, unit_tiles)
        after = lax.div((i + 1) * count, unit_tiles)

        @pl.when(after > before)
        def _():
            service(w, first + before)

    gate_count = min(unit_tiles, events - early_value)

    @pl.loop(0, unit_tiles)
    def _(n):
        for to, cols, conv in up_tile(wg, cg_v, n):
            hid[to, cols] = (conv / (1.0 + jnp.exp(-conv))).astype(jnp.bfloat16)
        spread(1, early_value, gate_count, n)

    serve(1, early_value + gate_count, events)
    start_own(2)
    all_of_sib(1)
    down_count = min(unit_tiles, 3 * early)

    @pl.loop(0, unit_tiles)
    def _(n):
        for to, cols, conv in up_tile(wv, cv_v, n):
            hid[to, cols] = (hid[to, cols].astype(jnp.float32) * conv).astype(jnp.bfloat16)
        spread(2, 0, down_count, n)

    def sum_copy(h, d):
        return remote(
            send.at[h, d - 1], came.at[h, d - 1], sum_send.at[h, d], sum_recv.at[h, d], (sp, peer(d))
        )

    def out_copy(h, c):
        j = held(h) if c == 0 else sib_held(h)
        cols = pl.ds(mult(j * depth, depth), depth)
        return pltpu.make_async_copy(mid.at[:, cols], out.at[:, cols], out_sem.at[h, c])

    def finish_hop(h):
        for d in range(1, n_tp):
            got = came.at[h, d - 1]
            remote(
                got, got, sum_send.at[h, d], sum_recv.at[h, d], (sp, peer(d))
            ).wait_recv()
        for c in range(2):
            j = held(h) if c == 0 else sib_held(h)
            cols = pl.ds(mult(j * depth, depth), depth)
            from_cols = slice(c * depth, (c + 1) * depth)
            total = own[:, from_cols] + mid[:, cols].astype(jnp.float32)
            for d in range(1, n_tp):
                total = total + came[h, d - 1, :, from_cols].astype(jnp.float32)
            mid[:, cols] = total.astype(jnp.bfloat16)

    def down_rows(h, t):
        lhs = hid[pl.ds(mult(t * part, part), part), :]
        rhs = jnp.concatenate([wd[held(h)], wd[sib_held(h)]], axis=1)
        return jnp.dot(lhs, rhs, preferred_element_type=jnp.float32)

    @pl.loop(0, chips)
    def _(h):
        for s in range(SUB):

            @pl.when((h - 1) * SUB + s >= down_count)
            def _():
                service(2, (h - 1) * SUB + s)

        for s in range(SUB):
            sib_wait(2, h, s)
        for d in range(1, n_tp):
            send[h, d - 1] = down_rows(h, peer(d)).astype(jnp.bfloat16)

        @pl.when(h > 0)
        def _():
            finish_hop(h - 1)
            for c in range(2):
                out_copy(h - 1, c).start()

        own[...] = down_rows(h, tp)
        for d in range(1, n_tp):
            sum_copy(h, d).start()

    finish_hop(chips - 1)
    for c in range(2):
        out_copy(chips - 1, c).start()

    for copy in halos + heads_out + ow_out + ow_on + [nrm_halo]:
        copy.wait_send()

    @pl.loop(0, part_blocks)
    def _(i):
        for d in range(1, n_tp):
            nrm_copy(i, d).wait_send()

    for w in range(3):

        @pl.loop(0, chips)
        def _(h):
            for s in range(SUB):

                @pl.when(h > 0)
                def _():
                    ring_copy(w, h, s).wait_send()

                sib_copy(w, h, s).wait_send()

    @pl.loop(0, chips)
    def _(h):
        for d in range(1, n_tp):
            sum_copy(h, d).wait_send()
        for c in range(2):
            out_copy(h, c).wait()


def whole_layer(n_sp, n_tp, queries, keys, values, doc_ids, sinks, residual, out_weight,
                norm_gain, w_gate, w_value, conv_gate, conv_value, w_down):
    rows, q_width = queries.shape
    kv_width = keys.shape[1]
    part, width = residual.shape
    depth, units = w_gate.shape
    chips = n_sp // 2
    bf16, f32 = jnp.bfloat16, jnp.float32
    dma = pltpu.SemaphoreType.DMA
    part_blocks = part // WINDOW
    scratch = [
        pltpu.VMEM((width, units), bf16),
        pltpu.VMEM((width, units), bf16),
        pltpu.VMEM((n_sp, units, depth), bf16),
        pltpu.VMEM((HALO + rows, width), bf16),
        pltpu.VMEM((rows, units), bf16),
        pltpu.VMEM((HALO + rows, TILE), f32),
        pltpu.VMEM((rows, q_width), bf16),
        pltpu.VMEM((WINDOW + rows, kv_width), bf16),
        pltpu.VMEM((WINDOW + rows, kv_width), bf16),
        pltpu.VMEM((8 + rows // WINDOW, WINDOW), jnp.int32),
        pltpu.VMEM((8 + rows, WINDOW), jnp.int32),
        pltpu.VMEM((rows, WINDOW), f32),
        pltpu.VMEM((rows, WINDOW), f32),
        pltpu.VMEM((rows, q_width), bf16),
        pltpu.VMEM((n_tp - 1, part, q_width), bf16),
        pltpu.VMEM((n_tp, q_width, width), bf16),
        pltpu.VMEM((part, width), bf16),
        pltpu.VMEM((1, width), f32),
        pltpu.VMEM((3, units), f32),
        pltpu.VMEM((3, units), f32),
        pltpu.VMEM((chips, n_tp - 1, part, 2 * depth), bf16),
        pltpu.VMEM((chips, n_tp - 1, part, 2 * depth), bf16),
        pltpu.VMEM((part, 2 * depth), f32),
        dma((12,)),
        dma((3, chips, SUB)),
        dma((3, chips, SUB)),
        dma((3, chips, SUB)),
        dma((3, chips, SUB)),
        dma((4,)),
        dma((4,)),
        dma((2, n_tp)),
        dma((2, n_tp)),
        dma((n_tp,)),
        dma((n_tp,)),
        dma((part_blocks, n_tp)),
        dma((part_blocks, n_tp)),
        dma((chips, n_tp)),
        dma((chips, n_tp)),
        dma((chips, 2)),
    ]
    any_spec = pl.BlockSpec(memory_space=pl.ANY)
    specs = [any_spec] * 13
    specs[4] = pl.BlockSpec(memory_space=pltpu.SMEM)
    return pl.pallas_call(
        functools.partial(layer_kernel, n_sp, n_tp),
        out_shape=jax.ShapeDtypeStruct(residual.shape, residual.dtype),
        in_specs=specs,
        out_specs=any_spec,
        scratch_shapes=scratch,
        compiler_params=pltpu.CompilerParams(
            collective_id=0, has_side_effects=True, vmem_limit_bytes=VMEM_BYTES
        ),
    )(
        queries,
        keys,
        values,
        (doc_ids + 1).reshape(rows // WINDOW, WINDOW),
        sinks,
        residual,
        out_weight,
        norm_gain.reshape(1, width),
        w_gate,
        w_value,
        conv_gate,
        conv_value,
        w_down,
    )


def in_one_kernel(n_sp, n_tp, queries, keys, values, doc_ids, *weights):
    w_gate = weights[4]
    depth, units = w_gate.shape
    aligned = depth % 128 == 0 and keys.shape[1] % 128 == 0 and units % TILE == 0
    return aligned and n_sp % 4 == 0 and n_tp > 1 and doc_ids.shape[0] % (n_tp * WINDOW) == 0


def solution(mesh):
    n_sp, n_tp = mesh.shape["sp"], mesh.shape["tp"]

    def body(*args):
        if in_one_kernel(n_sp, n_tp, *args):
            return whole_layer(n_sp, n_tp, *args)
        return per_device(*args)

    return jax.shard_map(
        body,
        mesh=mesh,
        in_specs=(
            P("sp", "tp"),
            P("sp", "tp"),
            P("sp", "tp"),
            P("sp"),
            P("tp"),
            P(("sp", "tp"), None),
            P("tp", None),
            P(),
            P("sp", "tp"),
            P("sp", "tp"),
            P(None, "tp"),
            P(None, "tp"),
            P("tp", "sp"),
        ),
        out_specs=P(("sp", "tp"), None),
        check_vma=False,
    )
```

profile of v0, /device:TPU:0, one launch (start us, length us, event | category | flops | bytes accessed | tf_op | source)
XLA Modules:
  0.0 232.3 jit_solution(13590754571615376416)
XLA Ops:
  0.0 1.3 add_bitcast_fusion.docs
  1.3 227.8 %shard_map.127 = bf16[512,2048]{1,0:T(8,128)(2,1)} custom-call(bf16[1024,512]{1,0:T(8,128)(2,1)} %queries.1, bf16[1024,128]{1,0:T(8,128)(2,1)} %keys.1, bf16[1024,128]{1,0:T(8,128)(2,1)} %values.1, s32[8,128]{1,0:T(8,128)} %add_bitcast_fusion.docs, f32[8]{0:T(128)} %sinks.1, bf16[512,2048]{1,0:T(8,128)(2,1)} %residual.1, bf16[512,2048]{1,0:T(8,128)(2,1)} %out_weight.1, ...), custom_call_target="tpu_custom_call" | custom-call | tf_op jit(solution)/shard_map/pallas_call | solution.py:894
  229.1 3.2 %copy.15 = bf16[512,2048]{1,0:T(8,128)(2,1)} copy(bf16[512,2048]{1,0:T(8,128)(2,1)} %shard_map.127) | data formatting | bytes 4194304
where the time goes:
time: 234 us; the launch traced here: 232 us
  Pallas kernels  228 us (97%)
  local copies, waits for them, and re-layouts  3.16 us (1%)
    pallas_call x1, Pallas kernels, whole_layer(): pl.pallas_call(functools.partial(layer_kernel, n_sp, n_tp), out_shape=jax...  228 us

commit v1 on v0

--- a/solution.py
+++ b/solution.py
@@ -11,7 +11,8 @@
 HEAD_DIM = 64
 WINDOW = 128
 ROW_TILE = 128
-SUB = 2
+SUB = 4
+EARLY = 2
 HALO = 16
 TILE = 256
 VMEM_BYTES = 67043328
@@ -473,6 +474,11 @@
                 ring_copy(w, h + 1, s).start()
 
         sib_copy(w, h, s).start()
+        if w < 2:
+
+            @pl.when(e == (chips - 2) * SUB - 1)
+            def _():
+                start_own(w + 1)
 
     def serve(w, first, last):
         if last > first:
@@ -498,7 +504,7 @@
     local = [
         pltpu.make_async_copy(src, dst, local_sem.at[i]) for i, (src, dst) in enumerate(local)
     ]
-    for copy in local:
+    for copy in local[:4]:
         copy.start()
 
     barrier = pltpu.get_barrier_semaphore()
@@ -531,6 +537,8 @@
     ]
     for copy in ow_out:
         copy.start()
+    for copy in local[4:]:
+        copy.start()
 
     for i in range(3):
         local[i].wait()
@@ -540,7 +548,7 @@
 
     lane = lax.broadcasted_iota(jnp.int32, (WINDOW, 2 * HEAD_DIM), 1)
     low_lane = lane < HEAD_DIM
-    doc_v[7:8, :] = jnp.where(sp == 0, 0, doc_v[7:8, :])
+    doc_v[7:8, :] = jnp.where(sp == 0, -1, doc_v[7:8, :])
     for b in range(-1, blocks):
         row = doc_v[8 + b : 9 + b, :]
         column = jnp.broadcast_to(row, (WINDOW, WINDOW)).T
@@ -596,11 +604,13 @@
                     low_lane, mixed[:WINDOW], mixed[WINDOW:]
                 ).astype(jnp.bfloat16)
 
-    early = events // 7
+    def due(share):
+        return events * share // 28
+
     pl.loop(0, blocks - part_blocks)(
         lambda i: attend_block(lax.rem((tp + 1) * part_blocks + i, blocks))
     )
-    serve(0, 0, early // 2)
+    serve(0, 0, due(3))
     pl.loop(0, part_blocks)(lambda i: attend_block(tp * part_blocks + i))
     heads_out = [
         remote(
@@ -614,8 +624,8 @@
     ]
     for copy in heads_out:
         copy.start()
-    before_proj = 3 * early
-    serve(0, early // 2, before_proj)
+    before_proj = due(14)
+    serve(0, due(3), before_proj)
 
     for i in range(4, 9):
         local[i].wait()
@@ -673,8 +683,7 @@
 
     after_proj = min(events, before_proj + part_blocks)
     serve(0, after_proj, events)
-    start_own(1)
-    early_value = 2 * early
+    early_value = due(14)
     serve(1, 0, early_value)
 
     @pl.loop(0, part_blocks)
@@ -704,20 +713,21 @@
     all_of_sib(0)
     nrm_halo.wait_recv()
 
-    half_rows = HALO + rows // 2
-
-    def up_tile(w_ref, taps, n):
+    def up_tile(w_ref, taps, n, base, lengths):
         cols = pl.ds(mult(n * TILE, TILE), TILE)
-        for lo, hi in ((0, half_rows), (half_rows, HALO + rows)):
-            pre[lo:hi, :] = (
-                jnp.dot(nrm[lo:hi, :], w_ref[:, cols], preferred_element_type=jnp.float32)
+        at = 0
+        for length in lengths:
+            lhs = nrm[pl.ds(mult(base + at, HALO), length), :]
+            pre[at : at + length, :] = (
+                jnp.dot(lhs, w_ref[:, cols], preferred_element_type=jnp.float32)
                 .astype(jnp.bfloat16)
                 .astype(jnp.float32)
             )
+            at += length
         tap = taps[:, cols]
-        for b in range(blocks):
+        for b in range((at - HALO) // WINDOW):
             at = HALO + b * WINDOW
-            to = slice(b * WINDOW, (b + 1) * WINDOW)
+            to = pl.ds(mult(base + b * WINDOW, WINDOW), WINDOW)
             one = jnp.concatenate([same_one[to, :]] * (TILE // WINDOW), axis=1)
             two = jnp.concatenate([same_two[to, :]] * (TILE // WINDOW), axis=1)
             conv = tap[2:3] * pre[at : at + WINDOW, :]
@@ -737,29 +747,38 @@
 
     @pl.loop(0, unit_tiles)
     def _(n):
-        for to, cols, conv in up_tile(wg, cg_v, n):
+        lengths = (HALO + rows // 2, rows // 2)
+        for to, cols, conv in up_tile(wg, cg_v, n, 0, lengths):
             hid[to, cols] = (conv / (1.0 + jnp.exp(-conv))).astype(jnp.bfloat16)
         spread(1, early_value, gate_count, n)
 
     serve(1, early_value + gate_count, events)
-    start_own(2)
     all_of_sib(1)
-    down_count = min(unit_tiles, 3 * early)
-
-    @pl.loop(0, unit_tiles)
-    def _(n):
-        for to, cols, conv in up_tile(wv, cv_v, n):
-            hid[to, cols] = (hid[to, cols].astype(jnp.float32) * conv).astype(jnp.bfloat16)
-        spread(2, 0, down_count, n)
+
+    def value_part(t, first, count):
+        @pl.loop(0, unit_tiles)
+        def _(n):
+            for to, cols, conv in up_tile(wv, cv_v, n, t * part, (HALO + part,)):
+                hid[to, cols] = (hid[to, cols].astype(jnp.float32) * conv).astype(
+                    jnp.bfloat16
+                )
+            spread(2, first, count, n)
 
     def sum_copy(h, d):
         return remote(
-            send.at[h, d - 1], came.at[h, d - 1], sum_send.at[h, d], sum_recv.at[h, d], (sp, peer(d))
+            send.at[h, d - 1],
+            came.at[h, d - 1],
+            sum_send.at[h, d],
+            sum_recv.at[h, d],
+            (sp, peer(d)),
         )
 
+    def hop_cols(h, c):
+        j = held(h) if c == 0 else sib_held(h)
+        return pl.ds(mult(j * depth, depth), depth)
+
     def out_copy(h, c):
-        j = held(h) if c == 0 else sib_held(h)
-        cols = pl.ds(mult(j * depth, depth), depth)
+        cols = hop_cols(h, c)
         return pltpu.make_async_copy(mid.at[:, cols], out.at[:, cols], out_sem.at[h, c])
 
     def finish_hop(h):
@@ -769,45 +788,65 @@
                 got, got, sum_send.at[h, d], sum_recv.at[h, d], (sp, peer(d))
             ).wait_recv()
         for c in range(2):
-            j = held(h) if c == 0 else sib_held(h)
-            cols = pl.ds(mult(j * depth, depth), depth)
+            cols = hop_cols(h, c)
             from_cols = slice(c * depth, (c + 1) * depth)
-            total = own[:, from_cols] + mid[:, cols].astype(jnp.float32)
+            total = own[h, :, from_cols] + mid[:, cols].astype(jnp.float32)
             for d in range(1, n_tp):
                 total = total + came[h, d - 1, :, from_cols].astype(jnp.float32)
             mid[:, cols] = total.astype(jnp.bfloat16)
+        for c in range(2):
+            out_copy(h, c).start()
 
     def down_rows(h, t):
         lhs = hid[pl.ds(mult(t * part, part), part), :]
         rhs = jnp.concatenate([wd[held(h)], wd[sib_held(h)]], axis=1)
         return jnp.dot(lhs, rhs, preferred_element_type=jnp.float32)
 
-    @pl.loop(0, chips)
-    def _(h):
-        for s in range(SUB):
-
-            @pl.when((h - 1) * SUB + s >= down_count)
-            def _():
-                service(2, (h - 1) * SUB + s)
-
+    def down_far(h):
         for s in range(SUB):
             sib_wait(2, h, s)
         for d in range(1, n_tp):
             send[h, d - 1] = down_rows(h, peer(d)).astype(jnp.bfloat16)
 
-        @pl.when(h > 0)
-        def _():
-            finish_hop(h - 1)
-            for c in range(2):
-                out_copy(h - 1, c).start()
-
-        own[...] = down_rows(h, tp)
+    def send_sums(h):
         for d in range(1, n_tp):
             sum_copy(h, d).start()
 
+    served = SUB
+    for d in range(1, n_tp):
+        value_part(peer(d), 0, served if d == 1 else 0)
+    for h in range(EARLY):
+        down_far(h)
+        if h > 0:
+            send_sums(h - 1)
+    more = due(6)
+    value_part(tp, served, more)
+    send_sums(EARLY - 1)
+    served += more
+
+    @pl.loop(EARLY, chips + EARLY)
+    def _(h):
+        @pl.when(h < chips)
+        def _():
+            for s in range(SUB):
+
+                @pl.when((h - 1) * SUB + s >= served)
+                def _():
+                    service(2, (h - 1) * SUB + s)
+
+            down_far(h)
+
+        own[h - EARLY] = down_rows(h - EARLY, tp)
+
+        @pl.when(h < chips)
+        def _():
+            send_sums(h)
+
+        @pl.when(h > EARLY)
+        def _():
+            finish_hop(h - EARLY - 1)
+
     finish_hop(chips - 1)
-    for c in range(2):
-        out_copy(chips - 1, c).start()
 
     for copy in halos + heads_out + ow_out + ow_on + [nrm_halo]:
         copy.wait_send()
@@ -870,7 +909,7 @@
         pltpu.VMEM((3, units), f32),
         pltpu.VMEM((chips, n_tp - 1, part, 2 * depth), bf16),
         pltpu.VMEM((chips, n_tp - 1, part, 2 * depth), bf16),
-        pltpu.VMEM((part, 2 * depth), f32),
+        pltpu.VMEM((chips, part, 2 * depth), f32),
         dma((12,)),
         dma((3, chips, SUB)),
         dma((3, chips, SUB)),
@@ -904,7 +943,7 @@
         queries,
         keys,
         values,
-        (doc_ids + 1).reshape(rows // WINDOW, WINDOW),
+        doc_ids.reshape(rows // WINDOW, WINDOW),
         sinks,
         residual,
         out_weight,

time: 234 us -> 196 us (0.84)
  Pallas kernels: 228 us -> 192 us
    pallas_call x1, Pallas kernels: 228 us -> 192 us  [whole_layer(): pl.pallas_call(functools.partial(layer_kernel, n_sp, n_tp), out_shape=jax...]
where the time goes in v1:
time: 196 us
  Pallas kernels  192 us (98%)
  local copies, waits for them, and re-layouts  3.16 us (2%)
    pallas_call x1, Pallas kernels, whole_layer(): pl.pallas_call(functools.partial(layer_kernel, n_sp, n_tp), out_shape=jax...  192 us

profile of v1, /device:TPU:0, one launch (start us, length us, event | category | flops | bytes accessed | tf_op | source)
XLA Modules:
  0.0 195.5 jit_solution(519447320341064412)
XLA Ops:
  0.0 192.3 %shard_map.127 = bf16[512,2048]{1,0:T(8,128)(2,1)} custom-call(bf16[1024,512]{1,0:T(8,128)(2,1)} %queries.1, bf16[1024,128]{1,0:T(8,128)(2,1)} %keys.1, bf16[1024,128]{1,0:T(8,128)(2,1)} %values.1, s32[8,128]{1,0:T(8,128)} %bitcast.3, f32[8]{0:T(128)} %sinks.1, bf16[512,2048]{1,0:T(8,128)(2,1)} %residual.1, bf16[512,2048]{1,0:T(8,128)(2,1)} %out_weight.1, ...), custom_call_target="tpu_custom_call" | custom-call | tf_op jit(solution)/shard_map/pallas_call | solution.py:933
  192.3 3.2 %copy.15 = bf16[512,2048]{1,0:T(8,128)(2,1)} copy(bf16[512,2048]{1,0:T(8,128)(2,1)} %shard_map.127) | data formatting | bytes 4194304

commit v2 on v1

--- a/solution.py
+++ b/solution.py
@@ -15,7 +15,7 @@
 EARLY = 2
 HALO = 16
 TILE = 256
-VMEM_BYTES = 67043328
+VMEM_BYTES = 64800000
 MESH = pl.DeviceIdType.MESH
 
 
@@ -324,7 +324,7 @@
     conv_gate,
     conv_value,
     w_down,
-    out,
+    mid,
     wg,
     wv,
     wd,
@@ -341,7 +341,6 @@
     att,
     heads,
     ow,
-    mid,
     gain_v,
     cg_v,
     cv_v,
@@ -363,7 +362,6 @@
     nrm_recv,
     sum_send,
     sum_recv,
-    out_sem,
 ):
     sp = lax.axis_index("sp")
     tp = lax.axis_index("tp")
@@ -427,7 +425,7 @@
         return remote(
             dst if src is None else src,
             dst,
-            ring_send.at[w, h, s],
+            ring_send.at[w],
             ring_recv.at[w, h, s],
             (down_sp, tp),
         )
@@ -435,24 +433,27 @@
     def ring_wait(w, h, s):
         dst = piece(w, held(h), s)
         remote(
-            dst, dst, ring_send.at[w, h, s], ring_recv.at[w, h, s], (down_sp, tp)
+            dst, dst, ring_send.at[w], ring_recv.at[w, h, s], (down_sp, tp)
         ).wait_recv()
+
+    def sib_sems(w, h):
+        return sib_send.at[w], sib_recv.at[w, h if w == 2 else 0]
 
     def sib_copy(w, h, s, src=None):
         dst = piece(w, held(h), s)
-        return remote(
-            dst if src is None else src,
-            dst,
-            sib_send.at[w, h, s],
-            sib_recv.at[w, h, s],
-            (sib_sp, tp),
-        )
-
-    def sib_wait(w, h, s):
-        dst = piece(w, sib_held(h), s)
-        remote(
-            dst, dst, sib_send.at[w, h, s], sib_recv.at[w, h, s], (sib_sp, tp)
-        ).wait_recv()
+        return remote(dst if src is None else src, dst, *sib_sems(w, h), (sib_sp, tp))
+
+    def sib_wait(w, h):
+        got = wd.at[sib_held(h)] if w == 2 else (wg, wv)[w].at[pl.ds(0, chips * depth), :]
+        remote(got, got, *sib_sems(w, h), (sib_sp, tp)).wait_recv()
+
+    def sent_weights(w):
+        passed = (chips - 1) * depth
+        buf = (wg, wv, wd)[w]
+        ring = buf.at[pl.ds(0, chips - 1)] if w == 2 else buf.at[pl.ds(0, passed), :]
+        swapped = buf.at[pl.ds(0, chips)] if w == 2 else buf.at[pl.ds(0, chips * depth), :]
+        remote(ring, ring, ring_send.at[w], ring_recv.at[w, 0, 0], (down_sp, tp)).wait_send()
+        remote(swapped, swapped, *sib_sems(w, 0), (sib_sp, tp)).wait_send()
 
     def start_own(w):
         for s in range(SUB):
@@ -648,7 +649,7 @@
 
     def nrm_copy(i, d):
         at = nrm_rows(tp, i)
-        return remote(at, at, nrm_send.at[i, d], nrm_recv.at[i, d], (sp, peer(n_tp - d)))
+        return remote(at, at, nrm_send.at[0], nrm_recv.at[i, d], (sp, peer(n_tp - d)))
 
     def project(i):
         at = pl.ds(mult(i * WINDOW, WINDOW), WINDOW)
@@ -666,34 +667,34 @@
         nrm[pl.ds(mult(HALO + part_base + i * WINDOW, HALO), WINDOW), :] = normed
 
     @pl.loop(0, part_blocks)
-    def _(i):
+    def _(k):
+        i = part_blocks - 1 - k
         project(i)
         for d in range(1, n_tp):
 
-            @pl.when(i > 0)
+            @pl.when(k > 0)
             def _():
-                nrm_copy(i - 1, d).start()
-
-        @pl.when(before_proj + i < events)
+                nrm_copy(i + 1, d).start()
+
+        @pl.when(before_proj + k < events)
         def _():
-            service(0, before_proj + i)
+            service(0, before_proj + k)
 
     for d in range(1, n_tp):
-        nrm_copy(part_blocks - 1, d).start()
+        nrm_copy(0, d).start()
 
     after_proj = min(events, before_proj + part_blocks)
     serve(0, after_proj, events)
     early_value = due(14)
-    serve(1, 0, early_value)
-
-    @pl.loop(0, part_blocks)
-    def _(i):
+
+    def nrm_wait(i):
         for d in range(1, n_tp):
             got = nrm_rows(peer(d), i)
             remote(
-                got, got, nrm_send.at[i, d], nrm_recv.at[i, d], (sp, peer(n_tp - d))
+                got, got, nrm_send.at[0], nrm_recv.at[i, d], (sp, peer(n_tp - d))
             ).wait_recv()
 
+    nrm_wait(part_blocks - 1)
     nrm_halo = remote(
         nrm.at[pl.ds(rows, HALO), :],
         nrm.at[pl.ds(0, HALO), :],
@@ -702,15 +703,18 @@
         (next_sp, tp),
     )
     nrm_halo.start()
+    serve(1, 0, early_value)
+    pl.loop(0, part_blocks - 1)(nrm_wait)
     for i in range(9, 12):
         local[i].wait()
 
-    def all_of_sib(w):
-        @pl.loop(0, chips * SUB)
-        def _(e):
-            sib_wait(w, lax.div(e, SUB), lax.rem(e, SUB))
-
-    all_of_sib(0)
+    sib_wait(0, 0)
+    for copy in halos + heads_out + ow_out + ow_on + [nrm_halo]:
+        copy.wait_send()
+
+    sent_rows = nrm.at[pl.ds(0, (n_tp - 1) * part), :]
+    remote(sent_rows, sent_rows, nrm_send.at[0], nrm_recv.at[0, 1], (sp, peer(1))).wait_send()
+
     nrm_halo.wait_recv()
 
     def up_tile(w_ref, taps, n, base, lengths):
@@ -753,7 +757,7 @@
         spread(1, early_value, gate_count, n)
 
     serve(1, early_value + gate_count, events)
-    all_of_sib(1)
+    sib_wait(1, 0)
 
     def value_part(t, first, count):
         @pl.loop(0, unit_tiles)
@@ -768,7 +772,7 @@
         return remote(
             send.at[h, d - 1],
             came.at[h, d - 1],
-            sum_send.at[h, d],
+            sum_send.at[0],
             sum_recv.at[h, d],
             (sp, peer(d)),
         )
@@ -776,16 +780,12 @@
     def hop_cols(h, c):
         j = held(h) if c == 0 else sib_held(h)
         return pl.ds(mult(j * depth, depth), depth)
-
-    def out_copy(h, c):
-        cols = hop_cols(h, c)
-        return pltpu.make_async_copy(mid.at[:, cols], out.at[:, cols], out_sem.at[h, c])
 
     def finish_hop(h):
         for d in range(1, n_tp):
             got = came.at[h, d - 1]
             remote(
-                got, got, sum_send.at[h, d], sum_recv.at[h, d], (sp, peer(d))
+                got, got, sum_send.at[0], sum_recv.at[h, d], (sp, peer(d))
             ).wait_recv()
         for c in range(2):
             cols = hop_cols(h, c)
@@ -794,8 +794,6 @@
             for d in range(1, n_tp):
                 total = total + came[h, d - 1, :, from_cols].astype(jnp.float32)
             mid[:, cols] = total.astype(jnp.bfloat16)
-        for c in range(2):
-            out_copy(h, c).start()
 
     def down_rows(h, t):
         lhs = hid[pl.ds(mult(t * part, part), part), :]
@@ -803,8 +801,7 @@
         return jnp.dot(lhs, rhs, preferred_element_type=jnp.float32)
 
     def down_far(h):
-        for s in range(SUB):
-            sib_wait(2, h, s)
+        sib_wait(2, h)
         for d in range(1, n_tp):
             send[h, d - 1] = down_rows(h, peer(d)).astype(jnp.bfloat16)
 
@@ -812,16 +809,20 @@
         for d in range(1, n_tp):
             sum_copy(h, d).start()
 
-    served = SUB
+    served = due(5)
     for d in range(1, n_tp):
         value_part(peer(d), 0, served if d == 1 else 0)
-    for h in range(EARLY):
+
+    @pl.loop(0, EARLY)
+    def _(h):
         down_far(h)
-        if h > 0:
-            send_sums(h - 1)
+        for i in range(due(1)):
+            service(2, served + h * due(1) + i)
+        send_sums(h)
+
+    served += EARLY * due(1)
     more = due(6)
     value_part(tp, served, more)
-    send_sums(EARLY - 1)
     served += more
 
     @pl.loop(EARLY, chips + EARLY)
@@ -836,44 +837,27 @@
 
             down_far(h)
 
-        own[h - EARLY] = down_rows(h - EARLY, tp)
+        @pl.when(h > EARLY)
+        def _():
+            finish_hop(h - EARLY - 1)
+
+        for w in range(2):
+
+            @pl.when(h == EARLY + w)
+            def _():
+                sent_weights(w)
 
         @pl.when(h < chips)
         def _():
             send_sums(h)
 
-        @pl.when(h > EARLY)
-        def _():
-            finish_hop(h - EARLY - 1)
+        own[h - EARLY] = down_rows(h - EARLY, tp)
 
     finish_hop(chips - 1)
 
-    for copy in halos + heads_out + ow_out + ow_on + [nrm_halo]:
-        copy.wait_send()
-
-    @pl.loop(0, part_blocks)
-    def _(i):
-        for d in range(1, n_tp):
-            nrm_copy(i, d).wait_send()
-
-    for w in range(3):
-
-        @pl.loop(0, chips)
-        def _(h):
-            for s in range(SUB):
-
-                @pl.when(h > 0)
-                def _():
-                    ring_copy(w, h, s).wait_send()
-
-                sib_copy(w, h, s).wait_send()
-
-    @pl.loop(0, chips)
-    def _(h):
-        for d in range(1, n_tp):
-            sum_copy(h, d).wait_send()
-        for c in range(2):
-            out_copy(h, c).wait()
+    sent_weights(2)
+
+    remote(send, send, sum_send.at[0], sum_recv.at[0, 1], (sp, peer(1))).wait_send()
 
 
 def whole_layer(n_sp, n_tp, queries, keys, values, doc_ids, sinks, residual, out_weight,
@@ -903,7 +887,6 @@
         pltpu.VMEM((rows, q_width), bf16),
         pltpu.VMEM((n_tp - 1, part, q_width), bf16),
         pltpu.VMEM((n_tp, q_width, width), bf16),
-        pltpu.VMEM((part, width), bf16),
         pltpu.VMEM((1, width), f32),
         pltpu.VMEM((3, units), f32),
         pltpu.VMEM((3, units), f32),
@@ -911,30 +894,29 @@
         pltpu.VMEM((chips, n_tp - 1, part, 2 * depth), bf16),
         pltpu.VMEM((chips, part, 2 * depth), f32),
         dma((12,)),
+        dma((3,)),
         dma((3, chips, SUB)),
-        dma((3, chips, SUB)),
-        dma((3, chips, SUB)),
-        dma((3, chips, SUB)),
+        dma((3,)),
+        dma((3, chips)),
         dma((4,)),
         dma((4,)),
         dma((2, n_tp)),
         dma((2, n_tp)),
         dma((n_tp,)),
         dma((n_tp,)),
+        dma((1,)),
         dma((part_blocks, n_tp)),
-        dma((part_blocks, n_tp)),
+        dma((1,)),
         dma((chips, n_tp)),
-        dma((chips, n_tp)),
-        dma((chips, 2)),
     ]
     any_spec = pl.BlockSpec(memory_space=pl.ANY)
     specs = [any_spec] * 13
     specs[4] = pl.BlockSpec(memory_space=pltpu.SMEM)
     return pl.pallas_call(
         functools.partial(layer_kernel, n_sp, n_tp),
-        out_shape=jax.ShapeDtypeStruct(residual.shape, residual.dtype),
+        out_shape=pltpu.VMEM(residual.shape, residual.dtype),
         in_specs=specs,
-        out_specs=any_spec,
+        out_specs=pl.BlockSpec(memory_space=pltpu.VMEM),
         scratch_shapes=scratch,
         compiler_params=pltpu.CompilerParams(
             collective_id=0, has_side_effects=True, vmem_limit_bytes=VMEM_BYTES

time: 196 us -> 184 us (0.939)
  Pallas kernels: 192 us -> 182 us
    pallas_call x1, Pallas kernels: 192 us -> 182 us  [whole_layer(): pl.pallas_call(functools.partial(layer_kernel, n_sp, n_tp), out_shape=plt...]
where the time goes in v2:
time: 184 us
  Pallas kernels  182 us (99%)
    pallas_call x1, Pallas kernels, whole_layer(): pl.pallas_call(functools.partial(layer_kernel, n_sp, n_tp), out_shape=plt...  182 us

profile of v2, /device:TPU:0, one launch (start us, length us, event | category | flops | bytes accessed | tf_op | source)
XLA Modules:
  0.0 183.6 jit_solution(11264622008291232885)
XLA Ops:
  0.0 182.3 %shard_map.127 = bf16[512,2048]{1,0:T(8,128)(2,1)S(1)} custom-call(bf16[1024,512]{1,0:T(8,128)(2,1)} %queries.1, bf16[1024,128]{1,0:T(8,128)(2,1)} %keys.1, bf16[1024,128]{1,0:T(8,128)(2,1)} %values.1, s32[8,128]{1,0:T(8,128)} %bitcast.3, f32[8]{0:T(128)} %sinks.1, bf16[512,2048]{1,0:T(8,128)(2,1)} %residual.1, bf16[512,2048]{1,0:T(8,128)(2,1)} %out_weight.1, ...), custom_call_target="tpu_custom_call" | custom-call | tf_op jit(solution)/shard_map/pallas_call | solution.py:915
  182.3 1.3 copy.15

commit v3 on v2

--- a/solution.py
+++ b/solution.py
@@ -398,17 +398,14 @@
         return 2 * ring_chip(lax.rem(place + way * h + chips, chips), chips) + 1 - core
 
     def piece(w, j, s):
+        size = depth // SUB
+        return (wg, wv, wd)[w].at[pl.ds(mult(j * depth + s * size, size), size), :]
+
+    def own_piece(w, s):
         if w == 2:
-            size = units // SUB
-            return wd.at[j, pl.ds(mult(s * size, size), size), :]
+            return piece(2, sp, s)
         size = depth // SUB
-        buf = (wg, wv)[w]
-        return buf.at[pl.ds(mult(j * depth + s * size, size), size), :]
-
-    def own_piece(w, s):
-        ref = (w_gate, w_value, w_down)[w]
-        size = ref.shape[0] // SUB
-        return ref.at[pl.ds(s * size, size), :]
+        return (w_gate, w_value)[w].at[pl.ds(s * size, size), :]
 
     def remote(src, dst, send_sem, recv_sem, device):
         return pltpu.make_async_remote_copy(
@@ -436,24 +433,40 @@
             dst, dst, ring_send.at[w], ring_recv.at[w, h, s], (down_sp, tp)
         ).wait_recv()
 
-    def sib_sems(w, h):
-        return sib_send.at[w], sib_recv.at[w, h if w == 2 else 0]
+    def sib_sem(w, h, s):
+        if w < 2:
+            return sib_recv.at[w, 0]
+        late = lax.div(h, chips - 1) * (s // (SUB // 2) if isinstance(s, int) else lax.div(s, SUB // 2))
+        return sib_recv.at[w, h + late]
 
     def sib_copy(w, h, s, src=None):
         dst = piece(w, held(h), s)
-        return remote(dst if src is None else src, dst, *sib_sems(w, h), (sib_sp, tp))
-
-    def sib_wait(w, h):
-        got = wd.at[sib_held(h)] if w == 2 else (wg, wv)[w].at[pl.ds(0, chips * depth), :]
-        remote(got, got, *sib_sems(w, h), (sib_sp, tp)).wait_recv()
+        return remote(
+            dst if src is None else src, dst, sib_send.at[w], sib_sem(w, h, s), (sib_sp, tp)
+        )
+
+    def sib_wait(w, h, part_of=None):
+        buf = (wg, wv, wd)[w]
+        if w < 2:
+            got = buf.at[pl.ds(0, chips * depth), :]
+        elif part_of is None:
+            got = buf.at[pl.ds(mult(sib_held(h) * depth, depth), depth), :]
+        else:
+            got = last_half(sib_held(h), part_of)
+        sem = sib_sem(w, h, 0 if part_of is None else part_of * (SUB // 2))
+        remote(got, got, sib_send.at[w], sem, (sib_sp, tp)).wait_recv()
+
+    def last_half(j, part_of):
+        return wd.at[pl.ds(mult(j * depth + part_of * (depth // 2), depth // 2), depth // 2), :]
 
     def sent_weights(w):
-        passed = (chips - 1) * depth
         buf = (wg, wv, wd)[w]
-        ring = buf.at[pl.ds(0, chips - 1)] if w == 2 else buf.at[pl.ds(0, passed), :]
-        swapped = buf.at[pl.ds(0, chips)] if w == 2 else buf.at[pl.ds(0, chips * depth), :]
+        ring = buf.at[pl.ds(0, (chips - 1) * depth), :]
+        swapped = buf.at[pl.ds(0, chips * depth), :]
         remote(ring, ring, ring_send.at[w], ring_recv.at[w, 0, 0], (down_sp, tp)).wait_send()
-        remote(swapped, swapped, *sib_sems(w, 0), (sib_sp, tp)).wait_send()
+        remote(
+            swapped, swapped, sib_send.at[w], sib_recv.at[w, 0], (sib_sp, tp)
+        ).wait_send()
 
     def start_own(w):
         for s in range(SUB):
@@ -500,7 +513,14 @@
         (conv_value, cv_v),
         (w_gate, wg.at[pl.ds(mult(sp * depth, depth), depth), :]),
         (w_value, wv.at[pl.ds(mult(sp * depth, depth), depth), :]),
-        (w_down, wd.at[sp]),
+    ]
+    strips = [(c, min(rows, units - c * rows)) for c in range(-(-units // rows))]
+    local += [
+        (
+            w_down.at[pl.ds(c * rows, length), :],
+            hid.at[pl.ds(0, length), pl.ds(c * depth, depth)],
+        )
+        for c, length in strips
     ]
     local = [
         pltpu.make_async_copy(src, dst, local_sem.at[i]) for i, (src, dst) in enumerate(local)
@@ -625,6 +645,14 @@
     ]
     for copy in heads_out:
         copy.start()
+    for copy in local[9:]:
+        copy.wait()
+    own_rows = pl.ds(mult(sp * depth, depth), depth)
+    for c, length in strips:
+        for at in range(0, length, TILE):
+            turned_piece = hid[at : at + TILE, c * depth : (c + 1) * depth].astype(jnp.float32).T
+            to = slice(c * rows + at, c * rows + at + TILE)
+            wd[own_rows, to] = turned_piece.astype(jnp.bfloat16)
     before_proj = due(14)
     serve(0, due(3), before_proj)
 
@@ -705,8 +733,6 @@
     nrm_halo.start()
     serve(1, 0, early_value)
     pl.loop(0, part_blocks - 1)(nrm_wait)
-    for i in range(9, 12):
-        local[i].wait()
 
     sib_wait(0, 0)
     for copy in halos + heads_out + ow_out + ow_on + [nrm_halo]:
@@ -768,46 +794,90 @@
                 )
             spread(2, first, count, n)
 
-    def sum_copy(h, d):
-        return remote(
-            send.at[h, d - 1],
-            came.at[h, d - 1],
-            sum_send.at[0],
-            sum_recv.at[h, d],
-            (sp, peer(d)),
-        )
+    def sum_copy(h, d, half=None):
+        src, dst, sem = send.at[h, d - 1], came.at[h, d - 1], h
+        if half is not None:
+            lanes = slice(half * depth, (half + 1) * depth)
+            src, dst, sem = src.at[:, lanes], dst.at[:, lanes], h + half
+        return remote(src, dst, sum_send.at[0], sum_recv.at[sem, d], (sp, peer(d)))
 
     def hop_cols(h, c):
         j = held(h) if c == 0 else sib_held(h)
         return pl.ds(mult(j * depth, depth), depth)
 
+    def add_up(h, c, parts):
+        cols = hop_cols(h, c)
+        total = own[h, :, c * depth : (c + 1) * depth] + mid[:, cols].astype(jnp.float32)
+        for t in parts:
+            total = total + t.astype(jnp.float32)
+        mid[:, cols] = total.astype(jnp.bfloat16)
+
     def finish_hop(h):
         for d in range(1, n_tp):
-            got = came.at[h, d - 1]
-            remote(
-                got, got, sum_send.at[0], sum_recv.at[h, d], (sp, peer(d))
-            ).wait_recv()
+            sum_copy(h, d).wait_recv()
         for c in range(2):
-            cols = hop_cols(h, c)
-            from_cols = slice(c * depth, (c + 1) * depth)
-            total = own[h, :, from_cols] + mid[:, cols].astype(jnp.float32)
+            lanes = slice(c * depth, (c + 1) * depth)
+            add_up(h, c, [came[h, d - 1, :, lanes] for d in range(1, n_tp)])
+
+    def finish_last():
+        h = chips - 1
+        for half in range(2):
             for d in range(1, n_tp):
-                total = total + came[h, d - 1, :, from_cols].astype(jnp.float32)
-            mid[:, cols] = total.astype(jnp.bfloat16)
-
-    def down_rows(h, t):
+                sum_copy(h, d, half).wait_recv()
+        for c in range(2):
+            lo = c * (depth // 2)
+            pairs = [
+                [came[h, d - 1, :, at + lo : at + lo + depth // 2] for at in (0, depth)]
+                for d in range(1, n_tp)
+            ]
+            add_up(h, c, [jnp.concatenate(pair, axis=1) for pair in pairs])
+
+    def apart(step):
+        pl.when(sp >= 0)(step)
+
+    def down_rows(rhs, t):
         lhs = hid[pl.ds(mult(t * part, part), part), :]
-        rhs = jnp.concatenate([wd[held(h)], wd[sib_held(h)]], axis=1)
-        return jnp.dot(lhs, rhs, preferred_element_type=jnp.float32)
+        return lax.dot_general(
+            lhs, rhs, (((1,), (1,)), ((), ())), preferred_element_type=jnp.float32
+        )
+
+    def hop_rows(h):
+        return jnp.concatenate(
+            [wd[pl.ds(mult(j * depth, depth), depth), :] for j in (held(h), sib_held(h))], axis=0
+        )
 
     def down_far(h):
         sib_wait(2, h)
         for d in range(1, n_tp):
-            send[h, d - 1] = down_rows(h, peer(d)).astype(jnp.bfloat16)
-
-    def send_sums(h):
+
+            @apart
+            def _():
+                send[h, d - 1] = down_rows(hop_rows(h), peer(d)).astype(jnp.bfloat16)
+
+    def down_own(h):
+        @apart
+        def _():
+            own[h] = down_rows(hop_rows(h), tp)
+
+    def down_far_half(half):
+        h = chips - 1
+        sib_wait(2, h, half)
+
+        def rhs():
+            return jnp.concatenate(
+                [last_half(j, half)[...] for j in (held(h), sib_held(h))], axis=0
+            )
+
+        lanes = slice(half * depth, (half + 1) * depth)
         for d in range(1, n_tp):
-            sum_copy(h, d).start()
+
+            @apart
+            def _():
+                send[h, d - 1, :, lanes] = down_rows(rhs(), peer(d)).astype(jnp.bfloat16)
+
+    def send_sums(h, half=None):
+        for d in range(1, n_tp):
+            sum_copy(h, d, half).start()
 
     served = due(5)
     for d in range(1, n_tp):
@@ -825,17 +895,15 @@
     value_part(tp, served, more)
     served += more
 
-    @pl.loop(EARLY, chips + EARLY)
+    @pl.loop(EARLY, chips - 1)
     def _(h):
-        @pl.when(h < chips)
-        def _():
-            for s in range(SUB):
-
-                @pl.when((h - 1) * SUB + s >= served)
-                def _():
-                    service(2, (h - 1) * SUB + s)
-
-            down_far(h)
+        for s in range(SUB):
+
+            @pl.when((h - 1) * SUB + s >= served)
+            def _():
+                service(2, (h - 1) * SUB + s)
+
+        down_far(h)
 
         @pl.when(h > EARLY)
         def _():
@@ -847,13 +915,22 @@
             def _():
                 sent_weights(w)
 
-        @pl.when(h < chips)
-        def _():
-            send_sums(h)
-
-        own[h - EARLY] = down_rows(h - EARLY, tp)
-
-    finish_hop(chips - 1)
+        send_sums(h)
+        down_own(h - EARLY)
+
+    last = chips - 1
+    for half in range(2):
+        for s in range(SUB // 2):
+            service(2, (last - 1) * SUB + half * (SUB // 2) + s)
+        down_far_half(half)
+        finish_hop(last - EARLY - 1 + half)
+        send_sums(last, half)
+        down_own(last - EARLY + half)
+    for h in range(last - EARLY + 2, chips):
+        down_own(h)
+    for h in range(last - EARLY + 1, last):
+        finish_hop(h)
+    finish_last()
 
     sent_weights(2)
 
@@ -873,7 +950,7 @@
     scratch = [
         pltpu.VMEM((width, units), bf16),
         pltpu.VMEM((width, units), bf16),
-        pltpu.VMEM((n_sp, units, depth), bf16),
+        pltpu.VMEM((width, units), bf16),
         pltpu.VMEM((HALO + rows, width), bf16),
         pltpu.VMEM((rows, units), bf16),
         pltpu.VMEM((HALO + rows, TILE), f32),
@@ -893,11 +970,11 @@
         pltpu.VMEM((chips, n_tp - 1, part, 2 * depth), bf16),
         pltpu.VMEM((chips, n_tp - 1, part, 2 * depth), bf16),
         pltpu.VMEM((chips, part, 2 * depth), f32),
-        dma((12,)),
+        dma((11 - (-units // rows),)),
         dma((3,)),
         dma((3, chips, SUB)),
         dma((3,)),
-        dma((3, chips)),
+        dma((3, chips + 1)),
         dma((4,)),
         dma((4,)),
         dma((2, n_tp)),
@@ -907,7 +984,7 @@
         dma((1,)),
         dma((part_blocks, n_tp)),
         dma((1,)),
-        dma((chips, n_tp)),
+        dma((chips + 1, n_tp)),
     ]
     any_spec = pl.BlockSpec(memory_space=pl.ANY)
     specs = [any_spec] * 13

time: 184 us -> 182 us (0.989)
  no operation moved by 1% of the time
where the time goes in v3:
time: 182 us
  Pallas kernels  181 us (99%)
    pallas_call x1, Pallas kernels, whole_layer(): pl.pallas_call(functools.partial(layer_kernel, n_sp, n_tp), out_shape=plt...  181 us

profile of v3, /device:TPU:0, one launch (start us, length us, event | category | flops | bytes accessed | tf_op | source)
XLA Modules:
  0.0 182.3 jit_solution(11621844810207064827)
XLA Ops:
  0.0 181.0 %shard_map.127 = bf16[512,2048]{1,0:T(8,128)(2,1)S(1)} custom-call(bf16[1024,512]{1,0:T(8,128)(2,1)} %queries.1, bf16[1024,128]{1,0:T(8,128)(2,1)} %keys.1, bf16[1024,128]{1,0:T(8,128)(2,1)} %values.1, s32[8,128]{1,0:T(8,128)} %bitcast.3, f32[8]{0:T(128)} %sinks.1, bf16[512,2048]{1,0:T(8,128)(2,1)} %residual.1, bf16[512,2048]{1,0:T(8,128)(2,1)} %out_weight.1, ...), custom_call_target="tpu_custom_call" | custom-call | tf_op jit(solution)/shard_map/pallas_call | solution.py:992
  181.0 1.3 copy.15

commit v4 on v3

--- a/solution.py
+++ b/solution.py
@@ -14,6 +14,7 @@
 SUB = 4
 EARLY = 2
 HALO = 16
+REACH = 2
 TILE = 256
 VMEM_BYTES = 64800000
 MESH = pl.DeviceIdType.MESH
@@ -380,6 +381,7 @@
     rows, q_width = queries.shape
     part = rows // n_tp
     depth, units = w_gate.shape
+    width = residual.shape[1]
     kv_heads = keys.shape[1] // HEAD_DIM
     group = q_width // keys.shape[1]
     blocks = rows // WINDOW
@@ -423,21 +425,21 @@
             dst if src is None else src,
             dst,
             ring_send.at[w],
-            ring_recv.at[w, h, s],
+            ring_recv.at[w, h - 1, s],
             (down_sp, tp),
         )
 
     def ring_wait(w, h, s):
         dst = piece(w, held(h), s)
         remote(
-            dst, dst, ring_send.at[w], ring_recv.at[w, h, s], (down_sp, tp)
+            dst, dst, ring_send.at[w], ring_recv.at[w, h - 1, s], (down_sp, tp)
         ).wait_recv()
 
     def sib_sem(w, h, s):
         if w < 2:
-            return sib_recv.at[w, 0]
+            return sib_recv.at[w]
         late = lax.div(h, chips - 1) * (s // (SUB // 2) if isinstance(s, int) else lax.div(s, SUB // 2))
-        return sib_recv.at[w, h + late]
+        return sib_recv.at[2 + h + late]
 
     def sib_copy(w, h, s, src=None):
         dst = piece(w, held(h), s)
@@ -464,9 +466,7 @@
         ring = buf.at[pl.ds(0, (chips - 1) * depth), :]
         swapped = buf.at[pl.ds(0, chips * depth), :]
         remote(ring, ring, ring_send.at[w], ring_recv.at[w, 0, 0], (down_sp, tp)).wait_send()
-        remote(
-            swapped, swapped, sib_send.at[w], sib_recv.at[w, 0], (sib_sp, tp)
-        ).wait_send()
+        remote(swapped, swapped, sib_send.at[w], sib_recv.at[w], (sib_sp, tp)).wait_send()
 
     def start_own(w):
         for s in range(SUB):
@@ -528,6 +528,7 @@
     for copy in local[:4]:
         copy.start()
 
+    nrm[0:HALO, :] = jnp.zeros((HALO, width), jnp.bfloat16)
     barrier = pltpu.get_barrier_semaphore()
     greeted = [(down_sp, tp), (up_sp, tp), (sib_sp, tp), (next_sp, tp), (prev_sp, tp)]
     greeted += [(sp, peer(d)) for d in range(1, n_tp)]
@@ -553,7 +554,7 @@
 
     ow_src = out_weight.at[pl.ds(mult(core * ow_half, ow_half), ow_half), :]
     ow_out = [
-        remote(ow_src, ow_rows(tp, core), ow_send.at[0, d], ow_recv.at[0, d], (sp, peer(n_tp - d)))
+        remote(ow_src, ow_rows(tp, core), ow_send.at[0, d - 1], ow_recv.at[0, d - 1], (sp, peer(n_tp - d)))
         for d in range(1, n_tp)
     ]
     for copy in ow_out:
@@ -628,17 +629,26 @@
     def due(share):
         return events * share // 28
 
-    pl.loop(0, blocks - part_blocks)(
-        lambda i: attend_block(lax.rem((tp + 1) * part_blocks + i, blocks))
-    )
-    serve(0, 0, due(3))
-    pl.loop(0, part_blocks)(lambda i: attend_block(tp * part_blocks + i))
+    def attend_blocks(first, count, e, share):
+        @pl.loop(0, count)
+        def _(i):
+            attend_block(lax.rem(first + i, blocks))
+            before = lax.div(i * share, count)
+
+            @pl.when(lax.div((i + 1) * share, count) > before)
+            def _():
+                service(0, e + before)
+
+    far_share = min(due(2), blocks - part_blocks)
+    own_share = min(due(3), part_blocks)
+    attend_blocks((tp + 1) * part_blocks, blocks - part_blocks, 0, far_share)
+    attend_blocks(tp * part_blocks, part_blocks, far_share, own_share)
     heads_out = [
         remote(
             att.at[pl.ds(mult(peer(n_tp - d) * part, part), part), :],
             heads.at[d - 1],
-            heads_send.at[d],
-            heads_recv.at[d],
+            heads_send.at[d - 1],
+            heads_recv.at[d - 1],
             (sp, peer(n_tp - d)),
         )
         for d in range(1, n_tp)
@@ -653,21 +663,21 @@
             turned_piece = hid[at : at + TILE, c * depth : (c + 1) * depth].astype(jnp.float32).T
             to = slice(c * rows + at, c * rows + at + TILE)
             wd[own_rows, to] = turned_piece.astype(jnp.bfloat16)
-    before_proj = due(14)
-    serve(0, due(3), before_proj)
+    before_proj = due(16)
+    serve(0, far_share + own_share, before_proj)
 
     for i in range(4, 9):
         local[i].wait()
     ow_on = []
     for d in range(1, n_tp):
         got = ow_rows(peer(d), core)
-        remote(got, got, ow_send.at[0, d], ow_recv.at[0, d], (sp, peer(n_tp - d))).wait_recv()
-        copy = remote(got, got, ow_send.at[1, d], ow_recv.at[1, d], (sib_sp, tp))
+        remote(got, got, ow_send.at[0, d - 1], ow_recv.at[0, d - 1], (sp, peer(n_tp - d))).wait_recv()
+        copy = remote(got, got, ow_send.at[1, d - 1], ow_recv.at[1, d - 1], (sib_sp, tp))
         copy.start()
         ow_on.append(copy)
     for d in range(1, n_tp):
         got = ow_rows(peer(d), 1 - core)
-        remote(got, got, ow_send.at[1, d], ow_recv.at[1, d], (sib_sp, tp)).wait_recv()
+        remote(got, got, ow_send.at[1, d - 1], ow_recv.at[1, d - 1], (sib_sp, tp)).wait_recv()
         heads_out[d - 1].wait_recv()
 
     part_base = tp * part
@@ -677,7 +687,7 @@
 
     def nrm_copy(i, d):
         at = nrm_rows(tp, i)
-        return remote(at, at, nrm_send.at[0], nrm_recv.at[i, d], (sp, peer(n_tp - d)))
+        return remote(at, at, nrm_send.at[0], nrm_recv.at[i, d - 1], (sp, peer(n_tp - d)))
 
     def project(i):
         at = pl.ds(mult(i * WINDOW, WINDOW), WINDOW)
@@ -719,13 +729,13 @@
         for d in range(1, n_tp):
             got = nrm_rows(peer(d), i)
             remote(
-                got, got, nrm_send.at[0], nrm_recv.at[i, d], (sp, peer(n_tp - d))
+                got, got, nrm_send.at[0], nrm_recv.at[i, d - 1], (sp, peer(n_tp - d))
             ).wait_recv()
 
     nrm_wait(part_blocks - 1)
     nrm_halo = remote(
-        nrm.at[pl.ds(rows, HALO), :],
-        nrm.at[pl.ds(0, HALO), :],
+        nrm.at[pl.ds(HALO + rows - REACH, REACH), :],
+        nrm.at[pl.ds(HALO - REACH, REACH), :],
         halo_send.at[3],
         halo_recv.at[3],
         (next_sp, tp),
@@ -739,7 +749,7 @@
         copy.wait_send()
 
     sent_rows = nrm.at[pl.ds(0, (n_tp - 1) * part), :]
-    remote(sent_rows, sent_rows, nrm_send.at[0], nrm_recv.at[0, 1], (sp, peer(1))).wait_send()
+    remote(sent_rows, sent_rows, nrm_send.at[0], nrm_recv.at[0, 0], (sp, peer(1))).wait_send()
 
     nrm_halo.wait_recv()
 
@@ -799,7 +809,7 @@
         if half is not None:
             lanes = slice(half * depth, (half + 1) * depth)
             src, dst, sem = src.at[:, lanes], dst.at[:, lanes], h + half
-        return remote(src, dst, sum_send.at[0], sum_recv.at[sem, d], (sp, peer(d)))
+        return remote(src, dst, sum_send.at[0], sum_recv.at[sem, d - 1], (sp, peer(d)))
 
     def hop_cols(h, c):
         j = held(h) if c == 0 else sib_held(h)
@@ -934,7 +944,7 @@
 
     sent_weights(2)
 
-    remote(send, send, sum_send.at[0], sum_recv.at[0, 1], (sp, peer(1))).wait_send()
+    remote(send, send, sum_send.at[0], sum_recv.at[0, 0], (sp, peer(1))).wait_send()
 
 
 def whole_layer(n_sp, n_tp, queries, keys, values, doc_ids, sinks, residual, out_weight,
@@ -972,19 +982,19 @@
         pltpu.VMEM((chips, part, 2 * depth), f32),
         dma((11 - (-units // rows),)),
         dma((3,)),
-        dma((3, chips, SUB)),
+        dma((3, chips - 1, SUB)),
         dma((3,)),
-        dma((3, chips + 1)),
+        dma((chips + 3,)),
         dma((4,)),
         dma((4,)),
-        dma((2, n_tp)),
-        dma((2, n_tp)),
-        dma((n_tp,)),
-        dma((n_tp,)),
+        dma((2, n_tp - 1)),
+        dma((2, n_tp - 1)),
+        dma((n_tp - 1,)),
+        dma((n_tp - 1,)),
         dma((1,)),
-        dma((part_blocks, n_tp)),
+        dma((part_blocks, n_tp - 1)),
         dma((1,)),
-        dma((chips + 1, n_tp)),
+        dma((chips + 1, n_tp - 1)),
     ]
     any_spec = pl.BlockSpec(memory_space=pl.ANY)
     specs = [any_spec] * 13

time: 182 us -> 181 us (level)
  Pallas kernels: 181 us -> 179 us
where the time goes in v4:
time: 181 us
  Pallas kernels  179 us (99%)
    pallas_call x1, Pallas kernels, whole_layer(): pl.pallas_call(functools.partial(layer_kernel, n_sp, n_tp), out_shape=plt...  179 us

profile of v4, /device:TPU:0, one launch (start us, length us, event | category | flops | bytes accessed | tf_op | source)
XLA Modules:
  0.0 180.8 jit_solution(10005439963843232833)
XLA Ops:
  0.0 179.5 %shard_map.127 = bf16[512,2048]{1,0:T(8,128)(2,1)S(1)} custom-call(bf16[1024,512]{1,0:T(8,128)(2,1)} %queries.1, bf16[1024,128]{1,0:T(8,128)(2,1)} %keys.1, bf16[1024,128]{1,0:T(8,128)(2,1)} %values.1, s32[8,128]{1,0:T(8,128)} %bitcast.3, f32[8]{0:T(128)} %sinks.1, bf16[512,2048]{1,0:T(8,128)(2,1)} %residual.1, bf16[512,2048]{1,0:T(8,128)(2,1)} %out_weight.1, ...), custom_call_target="tpu_custom_call" | custom-call | tf_op jit(solution)/shard_map/pallas_call | solution.py:1002
  179.5 1.3 copy.15

commit v5 on v4

--- a/solution.py
+++ b/solution.py
@@ -16,7 +16,7 @@
 HALO = 16
 REACH = 2
 TILE = 256
-VMEM_BYTES = 64800000
+VMEM_BYTES = 67043328
 MESH = pl.DeviceIdType.MESH
 
 
@@ -342,6 +342,7 @@
     att,
     heads,
     ow,
+    sink_v,
     gain_v,
     cg_v,
     cv_v,
@@ -403,12 +404,6 @@
         size = depth // SUB
         return (wg, wv, wd)[w].at[pl.ds(mult(j * depth + s * size, size), size), :]
 
-    def own_piece(w, s):
-        if w == 2:
-            return piece(2, sp, s)
-        size = depth // SUB
-        return (w_gate, w_value)[w].at[pl.ds(s * size, size), :]
-
     def remote(src, dst, send_sem, recv_sem, device):
         return pltpu.make_async_remote_copy(
             src_ref=src,
@@ -419,15 +414,9 @@
             device_id_type=MESH,
         )
 
-    def ring_copy(w, h, s, src=None):
-        dst = piece(w, held(h - 1), s)
-        return remote(
-            dst if src is None else src,
-            dst,
-            ring_send.at[w],
-            ring_recv.at[w, h - 1, s],
-            (down_sp, tp),
-        )
+    def ring_copy(w, h, s):
+        at = piece(w, held(h - 1), s)
+        return remote(at, at, ring_send.at[w], ring_recv.at[w, h - 1, s], (down_sp, tp))
 
     def ring_wait(w, h, s):
         dst = piece(w, held(h), s)
@@ -441,11 +430,9 @@
         late = lax.div(h, chips - 1) * (s // (SUB // 2) if isinstance(s, int) else lax.div(s, SUB // 2))
         return sib_recv.at[2 + h + late]
 
-    def sib_copy(w, h, s, src=None):
-        dst = piece(w, held(h), s)
-        return remote(
-            dst if src is None else src, dst, sib_send.at[w], sib_sem(w, h, s), (sib_sp, tp)
-        )
+    def sib_copy(w, h, s):
+        at = piece(w, held(h), s)
+        return remote(at, at, sib_send.at[w], sib_sem(w, h, s), (sib_sp, tp))
 
     def sib_wait(w, h, part_of=None):
         buf = (wg, wv, wd)[w]
@@ -470,9 +457,9 @@
 
     def start_own(w):
         for s in range(SUB):
-            ring_copy(w, 1, s, own_piece(w, s)).start()
+            ring_copy(w, 1, s).start()
         for s in range(SUB):
-            sib_copy(w, 0, s, own_piece(w, s)).start()
+            sib_copy(w, 0, s).start()
 
     def service(w, e):
         h = 1 + (e // SUB if isinstance(e, int) else lax.div(e, SUB))
@@ -501,20 +488,22 @@
             def _(e):
                 service(w, e)
 
+    own_rows = pl.ds(mult(sp * depth, depth), depth)
+    strips = [(c, min(rows, units - c * rows)) for c in range(-(-units // rows))]
     local = [
+        (w_gate, wg.at[own_rows, :]),
         (keys, k_v.at[pl.ds(WINDOW, rows), :]),
         (values, v_v.at[pl.ds(WINDOW, rows), :]),
         (docs, doc_v.at[pl.ds(8, blocks), :]),
         (queries, q_v),
+        (sinks, sink_v),
         (residual, mid),
         (out_weight, ow.at[tp]),
         (norm_gain, gain_v),
         (conv_gate, cg_v),
         (conv_value, cv_v),
-        (w_gate, wg.at[pl.ds(mult(sp * depth, depth), depth), :]),
-        (w_value, wv.at[pl.ds(mult(sp * depth, depth), depth), :]),
+        (w_value, wv.at[own_rows, :]),
     ]
-    strips = [(c, min(rows, units - c * rows)) for c in range(-(-units // rows))]
     local += [
         (
             w_down.at[pl.ds(c * rows, length), :],
@@ -525,7 +514,7 @@
     local = [
         pltpu.make_async_copy(src, dst, local_sem.at[i]) for i, (src, dst) in enumerate(local)
     ]
-    for copy in local[:4]:
+    for copy in local[:6]:
         copy.start()
 
     nrm[0:HALO, :] = jnp.zeros((HALO, width), jnp.bfloat16)
@@ -547,6 +536,7 @@
     ]
     for copy in halos:
         copy.start()
+    local[0].wait()
     start_own(0)
 
     def ow_rows(t, c):
@@ -559,14 +549,13 @@
     ]
     for copy in ow_out:
         copy.start()
-    for copy in local[4:]:
+    for copy in local[6:]:
         copy.start()
 
-    for i in range(3):
-        local[i].wait()
+    for copy in local[1:6]:
+        copy.wait()
     for copy in halos:
         copy.wait_recv()
-    local[3].wait()
 
     lane = lax.broadcasted_iota(jnp.int32, (WINDOW, 2 * HEAD_DIM), 1)
     low_lane = lane < HEAD_DIM
@@ -616,7 +605,7 @@
                     split, kk, (((1,), (1,)), ((), ())), preferred_element_type=jnp.float32
                 ) * HEAD_DIM ** (-0.5)
                 scores = jnp.where(keep, scores, -1e30)
-                sink = jnp.where(first_rows, sinks[head], sinks[head + 1])
+                sink = jnp.where(first_rows, sink_v[head], sink_v[head + 1])
                 peak = jnp.maximum(jnp.max(scores, axis=1, keepdims=True), sink)
                 expd = jnp.exp(scores - peak)
                 total = jnp.sum(expd, axis=1, keepdims=True) + jnp.exp(sink - peak)
@@ -655,9 +644,8 @@
     ]
     for copy in heads_out:
         copy.start()
-    for copy in local[9:]:
+    for copy in local[6:]:
         copy.wait()
-    own_rows = pl.ds(mult(sp * depth, depth), depth)
     for c, length in strips:
         for at in range(0, length, TILE):
             turned_piece = hid[at : at + TILE, c * depth : (c + 1) * depth].astype(jnp.float32).T
@@ -666,8 +654,6 @@
     before_proj = due(16)
     serve(0, far_share + own_share, before_proj)
 
-    for i in range(4, 9):
-        local[i].wait()
     ow_on = []
     for d in range(1, n_tp):
         got = ow_rows(peer(d), core)
@@ -804,12 +790,19 @@
                 )
             spread(2, first, count, n)
 
-    def sum_copy(h, d, half=None):
+    def sum_copy(h, d, strip=None):
         src, dst, sem = send.at[h, d - 1], came.at[h, d - 1], h
-        if half is not None:
-            lanes = slice(half * depth, (half + 1) * depth)
-            src, dst, sem = src.at[:, lanes], dst.at[:, lanes], h + half
+        if strip is not None:
+            at, lanes = last_strips[strip]
+            src, dst, sem = src.at[at, lanes], dst.at[at, lanes], h + strip
         return remote(src, dst, sum_send.at[0], sum_recv.at[sem, d - 1], (sp, peer(d)))
+
+    low_cols, high_cols = slice(0, depth), slice(depth, 2 * depth)
+    last_strips = [
+        (slice(0, part), low_cols),
+        (slice(0, part // 2), high_cols),
+        (slice(part // 2, part), high_cols),
+    ]
 
     def hop_cols(h, c):
         j = held(h) if c == 0 else sib_held(h)
@@ -831,9 +824,9 @@
 
     def finish_last():
         h = chips - 1
-        for half in range(2):
+        for strip in range(3):
             for d in range(1, n_tp):
-                sum_copy(h, d, half).wait_recv()
+                sum_copy(h, d, strip).wait_recv()
         for c in range(2):
             lo = c * (depth // 2)
             pairs = [
@@ -845,8 +838,8 @@
     def apart(step):
         pl.when(sp >= 0)(step)
 
-    def down_rows(rhs, t):
-        lhs = hid[pl.ds(mult(t * part, part), part), :]
+    def down_rows(rhs, t, at=0, length=part):
+        lhs = hid[pl.ds(mult(t * part + at, length), length), :]
         return lax.dot_general(
             lhs, rhs, (((1,), (1,)), ((), ())), preferred_element_type=jnp.float32
         )
@@ -869,25 +862,27 @@
         def _():
             own[h] = down_rows(hop_rows(h), tp)
 
-    def down_far_half(half):
+    def down_far_strip(strip):
         h = chips - 1
-        sib_wait(2, h, half)
+        at, lanes = last_strips[strip]
+        half = min(strip, 1)
 
         def rhs():
             return jnp.concatenate(
                 [last_half(j, half)[...] for j in (held(h), sib_held(h))], axis=0
             )
 
-        lanes = slice(half * depth, (half + 1) * depth)
         for d in range(1, n_tp):
 
             @apart
             def _():
-                send[h, d - 1, :, lanes] = down_rows(rhs(), peer(d)).astype(jnp.bfloat16)
-
-    def send_sums(h, half=None):
+                send[h, d - 1, at, lanes] = down_rows(
+                    rhs(), peer(d), at.start, at.stop - at.start
+                ).astype(jnp.bfloat16)
+
+    def send_sums(h, strip=None):
         for d in range(1, n_tp):
-            sum_copy(h, d, half).start()
+            sum_copy(h, d, strip).start()
 
     served = due(5)
     for d in range(1, n_tp):
@@ -929,17 +924,29 @@
         down_own(h - EARLY)
 
     last = chips - 1
-    for half in range(2):
+
+    def serve_last(half):
         for s in range(SUB // 2):
             service(2, (last - 1) * SUB + half * (SUB // 2) + s)
-        down_far_half(half)
-        finish_hop(last - EARLY - 1 + half)
-        send_sums(last, half)
-        down_own(last - EARLY + half)
-    for h in range(last - EARLY + 2, chips):
-        down_own(h)
-    for h in range(last - EARLY + 1, last):
-        finish_hop(h)
+        sib_wait(2, last, half)
+
+    def finish_range(first, stop):
+        for h in range(first, stop):
+            finish_hop(h)
+
+    serve_last(0)
+    down_far_strip(0)
+    finish_range(last - EARLY - 1, last - EARLY)
+    send_sums(last, 0)
+    pl.loop(last - EARLY, last)(down_own)
+    serve_last(1)
+    down_far_strip(1)
+    finish_range(last - EARLY, last - 1)
+    send_sums(last, 1)
+    down_far_strip(2)
+    finish_range(last - 1, last)
+    send_sums(last, 2)
+    down_own(last)
     finish_last()
 
     sent_weights(2)
@@ -974,13 +981,14 @@
         pltpu.VMEM((rows, q_width), bf16),
         pltpu.VMEM((n_tp - 1, part, q_width), bf16),
         pltpu.VMEM((n_tp, q_width, width), bf16),
+        pltpu.SMEM((q_width // HEAD_DIM,), f32),
         pltpu.VMEM((1, width), f32),
         pltpu.VMEM((3, units), f32),
         pltpu.VMEM((3, units), f32),
         pltpu.VMEM((chips, n_tp - 1, part, 2 * depth), bf16),
         pltpu.VMEM((chips, n_tp - 1, part, 2 * depth), bf16),
         pltpu.VMEM((chips, part, 2 * depth), f32),
-        dma((11 - (-units // rows),)),
+        dma((12 - (-units // rows),)),
         dma((3,)),
         dma((3, chips - 1, SUB)),
         dma((3,)),
@@ -994,19 +1002,17 @@
         dma((1,)),
         dma((part_blocks, n_tp - 1)),
         dma((1,)),
-        dma((chips + 1, n_tp - 1)),
+        dma((chips + 2, n_tp - 1)),
     ]
     any_spec = pl.BlockSpec(memory_space=pl.ANY)
-    specs = [any_spec] * 13
-    specs[4] = pl.BlockSpec(memory_space=pltpu.SMEM)
     return pl.pallas_call(
         functools.partial(layer_kernel, n_sp, n_tp),
         out_shape=pltpu.VMEM(residual.shape, residual.dtype),
-        in_specs=specs,
+        in_specs=[any_spec] * 13,
         out_specs=pl.BlockSpec(memory_space=pltpu.VMEM),
         scratch_shapes=scratch,
         compiler_params=pltpu.CompilerParams(
-            collective_id=0, has_side_effects=True, vmem_limit_bytes=VMEM_BYTES
+            collective_id=0, has_side_effects=True, vmem_limit_bytes=VMEM_BYTES - 2 * residual.size
         ),
     )(
         queries,

time: 181 us -> 180 us (level)
  no operation moved by 1% of the time
where the time goes in v5:
time: 180 us
  Pallas kernels  179 us (99%)
    pallas_call x1, Pallas kernels, whole_layer(): pl.pallas_call(functools.partial(layer_kernel, n_sp, n_tp), out_shape=plt...  179 us

profile of v5, /device:TPU:0, one launch (start us, length us, event | category | flops | bytes accessed | tf_op | source)
XLA Modules:
  0.0 180.2 jit_solution(9804474796404536269)
XLA Ops:
  0.0 178.9 %shard_map.127 = bf16[512,2048]{1,0:T(8,128)(2,1)S(1)} custom-call(bf16[1024,512]{1,0:T(8,128)(2,1)} %queries.1, bf16[1024,128]{1,0:T(8,128)(2,1)} %keys.1, bf16[1024,128]{1,0:T(8,128)(2,1)} %values.1, s32[8,128]{1,0:T(8,128)} %bitcast.3, f32[8]{0:T(128)} %sinks.1, bf16[512,2048]{1,0:T(8,128)(2,1)} %residual.1, bf16[512,2048]{1,0:T(8,128)(2,1)} %out_weight.1, ...), custom_call_target="tpu_custom_call" | custom-call | tf_op jit(solution)/shard_map/pallas_call | solution.py:1008
  178.9 1.3 copy.15

commit v6 on v5

--- a/solution.py
+++ b/solution.py
@@ -490,8 +490,9 @@
 
     own_rows = pl.ds(mult(sp * depth, depth), depth)
     strips = [(c, min(rows, units - c * rows)) for c in range(-(-units // rows))]
-    local = [
-        (w_gate, wg.at[own_rows, :]),
+    size = depth // SUB
+    local = [(w_gate.at[pl.ds(s * size, size), :], piece(0, sp, s)) for s in range(SUB)]
+    local += [
         (keys, k_v.at[pl.ds(WINDOW, rows), :]),
         (values, v_v.at[pl.ds(WINDOW, rows), :]),
         (docs, doc_v.at[pl.ds(8, blocks), :]),
@@ -514,7 +515,8 @@
     local = [
         pltpu.make_async_copy(src, dst, local_sem.at[i]) for i, (src, dst) in enumerate(local)
     ]
-    for copy in local[:6]:
+    early_end = SUB + 5
+    for copy in local[:early_end]:
         copy.start()
 
     nrm[0:HALO, :] = jnp.zeros((HALO, width), jnp.bfloat16)
@@ -536,8 +538,11 @@
     ]
     for copy in halos:
         copy.start()
-    local[0].wait()
-    start_own(0)
+    for s in range(SUB):
+        local[s].wait()
+        ring_copy(0, 1, s).start()
+    for s in range(SUB):
+        sib_copy(0, 0, s).start()
 
     def ow_rows(t, c):
         return ow.at[t, pl.ds(mult(c * ow_half, ow_half), ow_half), :]
@@ -549,10 +554,10 @@
     ]
     for copy in ow_out:
         copy.start()
-    for copy in local[6:]:
+    for copy in local[early_end:]:
         copy.start()
 
-    for copy in local[1:6]:
+    for copy in local[SUB:early_end]:
         copy.wait()
     for copy in halos:
         copy.wait_recv()
@@ -644,7 +649,7 @@
     ]
     for copy in heads_out:
         copy.start()
-    for copy in local[6:]:
+    for copy in local[early_end:]:
         copy.wait()
     for c, length in strips:
         for at in range(0, length, TILE):
@@ -988,7 +993,7 @@
         pltpu.VMEM((chips, n_tp - 1, part, 2 * depth), bf16),
         pltpu.VMEM((chips, n_tp - 1, part, 2 * depth), bf16),
         pltpu.VMEM((chips, part, 2 * depth), f32),
-        dma((12 - (-units // rows),)),
+        dma((11 + SUB - (-units // rows),)),
         dma((3,)),
         dma((3, chips - 1, SUB)),
         dma((3,)),

time: 180 us -> 180 us (level)
  no operation moved by 1% of the time
where the time goes in v6:
time: 180 us
  Pallas kernels  179 us (99%)
    pallas_call x1, Pallas kernels, whole_layer(): pl.pallas_call(functools.partial(layer_kernel, n_sp, n_tp), out_shape=plt...  179 us

profile of v6, /device:TPU:0, one launch (start us, length us, event | category | flops | bytes accessed | tf_op | source)
XLA Modules:
  0.0 180.2 jit_solution(12340486593854027315)
XLA Ops:
  0.0 178.9 %shard_map.127 = bf16[512,2048]{1,0:T(8,128)(2,1)S(1)} custom-call(bf16[1024,512]{1,0:T(8,128)(2,1)} %queries.1, bf16[1024,128]{1,0:T(8,128)(2,1)} %keys.1, bf16[1024,128]{1,0:T(8,128)(2,1)} %values.1, s32[8,128]{1,0:T(8,128)} %bitcast.3, f32[8]{0:T(128)} %sinks.1, bf16[512,2048]{1,0:T(8,128)(2,1)} %residual.1, bf16[512,2048]{1,0:T(8,128)(2,1)} %out_weight.1, ...), custom_call_target="tpu_custom_call" | custom-call | tf_op jit(solution)/shard_map/pallas_call | solution.py:1013
  178.9 1.3 copy.15
